TPU v7x, 256 devices: a whole 4x4x8 slice. The times are simulated.
256 devices in a mesh: sp: 64 (over z, x, core), tp: 4 (over y).
Axes of the slice: x: 4, y: 4, z: 8, core: 2. Of those that a mesh axis runs over, the one named last changes fastest.
Arguments:
- incoming_residual_stream: bfloat16 [32768, 2048], P(('sp', 'tp')), may hold values from -6 to 6
- result_valve: bfloat16 [32768, 2048], P('sp', 'tp'), may hold values from -6 to 6
- channel_feed_matrix: bfloat16 [32768, 2048], P('sp', 'tp'), may hold values from -6 to 6
- memory_feed_matrix: bfloat16 [32768, 512], P('sp', 'tp'), may hold values from -6 to 6
- memory_query_matrix: bfloat16 [32768, 512], P('sp', 'tp'), may hold values from -6 to 6
- unsoftened_deltas: float32 [32768, 32], P('sp', 'tp'), may hold values from -2.7 to 2.7
- delta_offset: float32 [32], P('tp'), may hold values from -4.5 to -3.5
- channel_fading_speed: float32 [32], P('tp'), as said below
- extra_log_fading: float32 [32768, 32], P('sp', 'tp'), may hold values from -0.7 to 0
- bypass_factor: float32 [32], P('tp'), may hold values from 0.1 to 1.9
- channel_feed_kernel: bfloat16 [4, 2048], P(None, 'tp'), may hold values from -3 to 3
- memory_feed_kernel: bfloat16 [4, 512], P(None, 'tp'), may hold values from -3 to 3
- memory_query_kernel: bfloat16 [4, 512], P(None, 'tp'), may hold values from -3 to 3
- cluster_scaling_vector: float32 [2048], P('tp'), may hold values from 0.1 to 1.9
- mixer_result_matrix: bfloat16 [2048, 2048], P('tp'), may hold values from -0.125 to 0.125
- initial_scaling_vector: float32 [2048], replicated, may hold values from 0.1 to 1.9
- valve_matrix: bfloat16 [2048, 5632], P('sp', 'tp'), may hold values from -0.125 to 0.125
- widen_matrix: bfloat16 [2048, 5632], P('sp', 'tp'), may hold values from -0.125 to 0.125
- shrink_matrix: bfloat16 [5632, 2048], P('tp', 'sp'), may hold values from -0.078125 to 0.078125
- valve_filter_kernel: bfloat16 [3, 5632], P(None, 'tp'), may hold values from -3.5 to 3.5
- widen_filter_kernel: bfloat16 [3, 5632], P(None, 'tp'), may hold values from -3.5 to 3.5
- latter_scaling_vector: float32 [2048], replicated, may hold values from 0.1 to 1.9
Outputs:
- layer_out: bfloat16 [32768, 2048], P(('sp', 'tp'))
Inputs may be any that keep to these rules, and one draw needn't show every extreme that they name: `channel_fading_speed`: positive.
All inputs are finite; a program needn't handle non-finite values.
Results may differ from a plain program's by a relative error of at most 0.02.
Values may be sent and summed in bfloat16 or wider, within the bound.
No kernel may reach another device: no remote copies, remote signals or barrier semaphores. Data moves between devices by JAX's collectives and lax.ppermute only.
A program may use at most 128 MiB of HBM per device.

v0:
```python
import jax
import jax.numpy as jnp
from jax import lax
from jax.sharding import Mesh
from jax.sharding import PartitionSpec as P

HEADS = 32
HEAD_DIM = 64
GROUPS = 4
STATE = 128
CONV = 4
FCONV = 3
BLOCK = 128
SP = ("sp_0", "sp_1", "sp_2")
SP_TP = ("sp_0", "sp_1", "sp_2", "tp")


EPSILON = 1e-05
ALPHA = 2.0**0.25


def gather_turned(arrays, axis, dims):
    turned = [jnp.moveaxis(a, dim, 0) for a, dim in zip(arrays, dims)]
    both = jnp.concatenate([t.reshape(len(t), -1) for t in turned], axis=1)
    out, at, finished = (lax.all_gather(both, axis, axis=0, tiled=True), 0, [])
    for t, dim in zip(turned, dims):
        slab = out[:, at : at + t[0].size].reshape(-1, *t.shape[1:])
        finished.append(jnp.moveaxis(slab, 0, dim))
        at += t[0].size
    return tuple(finished)


def shifted(shard, axis, by):
    count = lax.axis_size(axis)
    pairs = [(i, i + by) for i in range(count) if 0 <= i + by < count]
    return lax.ppermute(shard, axis, pairs)


def neutral_like(shard, identity):
    return jax.tree.map(
        lambda part, zero: jnp.zeros_like(part) + jnp.asarray(zero, part.dtype), shard, identity
    )


def entering(shard, axes, combine, identity):
    before = start = neutral_like(shard, identity)
    total = shard
    for axis in reversed(axes):
        count, place = (lax.axis_size(axis), lax.axis_index(axis))
        pieces = jax.tree.map(
            lambda part, kind: lax.all_gather(part.astype(kind), axis),
            total,
            (jnp.bfloat16, jnp.bfloat16),
        )
        inside, total = (start, start)
        for k in range(count):
            passed = k < place
            total = combine(
                total, jax.tree.map(lambda part, own: part[k].astype(own.dtype), pieces, shard)
            )
            inside = jax.tree.map(lambda new, old: jnp.where(passed, new, old), total, inside)
        before = combine(inside, before)
    return before


def in_blocks(shard, dim, count):
    before, after = (shard.shape[:dim], shard.shape[dim + 1 :])
    return jnp.moveaxis(shard.reshape(*before, count, -1, *after), dim, 0)


def sent_and_summed(shard, axis, dim):
    count = lax.axis_size(axis)
    pieces = lax.all_to_all(in_blocks(shard, dim, count), axis, 0, 0, tiled=True)
    return jnp.sum(pieces.astype(jnp.float32), axis=0)


def joined_along(pieces, dim):
    lengths = list(pieces.shape[1:])
    lengths[dim] *= pieces.shape[0]
    return jnp.moveaxis(pieces, 0, dim).reshape(lengths)


def sent_to_all(shard, axis):
    copies = jnp.broadcast_to(shard, (lax.axis_size(axis), *shard.shape))
    return lax.all_to_all(copies, axis, split_axis=0, concat_axis=0, tiled=True)


def gathered_copies(shard, axis, dim):
    return joined_along(sent_to_all(shard, axis), dim)


def causal_conv(signal, before, tap_weights):
    tap_count = tap_weights.shape[0]
    row_count = signal.shape[0]
    padded = jnp.concatenate([before, signal], axis=0).astype(jnp.float32)
    running = jnp.zeros(signal.shape, jnp.float32)
    for tap_index in range(tap_count):
        running = (
            running
            + tap_weights[tap_index].astype(jnp.float32) * padded[tap_index : tap_index + row_count]
        )
    return running


def layer_norm(values, scales):
    row_mean = jnp.mean(values, axis=-1, keepdims=True)
    centred = values - row_mean
    spread = jnp.mean(centred * centred, axis=-1, keepdims=True)
    return centred * lax.rsqrt(spread + EPSILON) * scales


def combine_states(earlier_pair, later_pair):
    return (
        earlier_pair[0] * later_pair[1][..., None, None] + later_pair[0],
        earlier_pair[1] * later_pair[1],
    )


def chain_step(state_now, inputs):
    fresh_one, decay_one = inputs
    return (state_now * decay_one[..., None, None] + fresh_one, state_now)


def shards(
    incoming_residual_stream,
    result_valve,
    channel_feed_matrix,
    memory_feed_matrix,
    memory_query_matrix,
    unsoftened_deltas,
    delta_offset,
    channel_fading_speed,
    extra_log_fading,
    bypass_factor,
    channel_feed_kernel,
    memory_feed_kernel,
    memory_query_kernel,
    cluster_scaling_vector,
    mixer_result_matrix,
    initial_scaling_vector,
    valve_matrix,
    widen_matrix,
    shrink_matrix,
    valve_filter_kernel,
    widen_filter_kernel,
    latter_scaling_vector,
):
    row_count = channel_feed_matrix.shape[0]
    inner_here = channel_feed_matrix.shape[1]
    group_count = memory_feed_matrix.shape[1] // STATE
    group_heads = HEADS // GROUPS
    block_count = row_count // BLOCK
    gate_whole, up_whole, down_whole = gather_turned(
        (valve_matrix, widen_matrix, shrink_matrix), SP, (0, 0, 1)
    )
    rim_rows = CONV - 1
    rim_x, rim_b, rim_c = shifted(
        (
            channel_feed_matrix[row_count - rim_rows :],
            memory_feed_matrix[row_count - rim_rows :],
            memory_query_matrix[row_count - rim_rows :],
        ),
        SP,
        1,
    )
    x_act = jax.nn.silu(causal_conv(channel_feed_matrix, rim_x, channel_feed_kernel)).astype(
        jnp.bfloat16
    )
    b_act = jax.nn.silu(causal_conv(memory_feed_matrix, rim_b, memory_feed_kernel)).astype(
        jnp.bfloat16
    )
    c_act = jax.nn.silu(causal_conv(memory_query_matrix, rim_c, memory_query_kernel)).astype(
        jnp.bfloat16
    )
    channel_delta_amount = jax.nn.softplus(unsoftened_deltas + delta_offset[None, :])
    log_fading_amount = extra_log_fading - channel_fading_speed[None, :] * channel_delta_amount
    x_heads = x_act.astype(jnp.float32).reshape(row_count, group_count, group_heads, HEAD_DIM)
    x_scaled = (
        x_heads * channel_delta_amount.reshape(row_count, group_count, group_heads)[..., None]
    )
    b_full = b_act.astype(jnp.float32).reshape(row_count, group_count, STATE)
    c_full = c_act.astype(jnp.float32).reshape(row_count, group_count, STATE)
    decay_full = log_fading_amount.reshape(row_count, group_count, group_heads)
    x_blk = x_scaled.reshape(block_count, BLOCK, group_count, group_heads, HEAD_DIM)
    b_blk = b_full.reshape(block_count, BLOCK, group_count, STATE)
    c_blk = c_full.reshape(block_count, BLOCK, group_count, STATE)
    b_narrow = b_act.reshape(block_count, BLOCK, group_count, STATE)
    c_narrow = c_act.reshape(block_count, BLOCK, group_count, STATE)
    decay_blk = decay_full.reshape(block_count, BLOCK, group_count, group_heads)
    cum_decay = jnp.cumsum(decay_blk, axis=1)
    causal = jnp.tril(jnp.ones((BLOCK, BLOCK), dtype=bool))
    between = cum_decay[:, :, None] - cum_decay[:, None, :]
    lag = jnp.exp(jnp.where(causal[None, :, :, None, None], between, -jnp.inf))
    affinity = jnp.einsum("blgn,bsgn->blsg", c_narrow, b_narrow, preferred_element_type=jnp.float32)
    mixing = affinity[..., None] * lag
    within = jnp.einsum("blsgh,bsghp->blghp", mixing, x_blk)
    to_end = jnp.exp(cum_decay[:, -1:] - cum_decay)
    fresh = jnp.einsum("blgn,blghp->bghpn", b_blk, x_blk * to_end[..., None])
    block_decay = jnp.exp(cum_decay[:, -1])
    initial = jnp.zeros((group_count, group_heads, HEAD_DIM, STATE), jnp.float32)
    local_end, earlier = lax.scan(chain_step, initial, (fresh, block_decay))
    carried = jnp.einsum("blgn,bghpn->blghp", c_blk, earlier) * jnp.exp(cum_decay)[..., None]
    from_start = jnp.cumsum(decay_full, axis=0)
    incoming, _ = entering(
        (local_end, jnp.exp(from_start[-1])),
        SP,
        combine_states,
        (jnp.zeros_like(local_end), jnp.ones_like(from_start[-1])),
    )
    arriving = jnp.einsum("tgn,ghpn->tghp", c_full, incoming) * jnp.exp(from_start)[..., None]
    y_heads = (within + carried).reshape(row_count, group_count, group_heads, HEAD_DIM) + arriving
    y_heads = y_heads + bypass_factor.reshape(group_count, group_heads)[None, :, :, None] * x_heads
    gated = y_heads.reshape(row_count, group_count, group_heads * HEAD_DIM)
    gated = gated * jax.nn.silu(result_valve.astype(jnp.float32)).reshape(
        row_count, group_count, group_heads * HEAD_DIM
    )
    gated = gated * lax.rsqrt(jnp.mean(gated * gated, axis=-1, keepdims=True) + EPSILON)
    y_norm = (gated.reshape(row_count, inner_here) * cluster_scaling_vector[None, :]).astype(
        jnp.bfloat16
    )
    mixer = sent_and_summed(
        jnp.dot(y_norm, mixer_result_matrix, preferred_element_type=jnp.float32).astype(
            jnp.bfloat16
        ),
        "tp",
        0,
    )
    normed_own = layer_norm(
        ALPHA * incoming_residual_stream.astype(jnp.float32) + mixer, initial_scaling_vector
    ).astype(jnp.bfloat16)
    normed_all = gathered_copies(normed_own, "tp", 0)
    gate_sum = jnp.dot(normed_all, gate_whole, preferred_element_type=jnp.float32)
    up_sum = jnp.dot(normed_all, up_whole, preferred_element_type=jnp.float32)
    gate_proj = gate_sum.astype(jnp.bfloat16)
    up_proj = up_sum.astype(jnp.bfloat16)
    ffn_rows = FCONV - 1
    rim_gate, rim_up = shifted(
        (gate_proj[row_count - ffn_rows :], up_proj[row_count - ffn_rows :]), SP, 1
    )
    gate_conv = causal_conv(gate_proj, rim_gate, valve_filter_kernel)
    up_conv = causal_conv(up_proj, rim_up, widen_filter_kernel)
    hidden = (jax.nn.silu(gate_conv) * up_conv).astype(jnp.bfloat16)
    channel_part = jnp.dot(hidden, down_whole, preferred_element_type=jnp.float32)
    channel = sent_and_summed(channel_part.astype(jnp.bfloat16), "tp", 0)
    return layer_norm(
        ALPHA * normed_own.astype(jnp.float32) + channel, latter_scaling_vector
    ).astype(jnp.bfloat16)


def solution(mesh):
    split = Mesh(mesh.devices.reshape(8, 4, 2, mesh.shape["tp"]), ("sp_0", "sp_1", "sp_2", "tp"))
    in_specs = (
        P(SP_TP, None),
        P(SP, "tp"),
        P(SP, "tp"),
        P(SP, "tp"),
        P(SP, "tp"),
        P(SP, "tp"),
        P("tp"),
        P("tp"),
        P(SP, "tp"),
        P("tp"),
        P(None, "tp"),
        P(None, "tp"),
        P(None, "tp"),
        P("tp"),
        P("tp", None),
        P(),
        P(SP, "tp"),
        P(SP, "tp"),
        P("tp", SP),
        P(None, "tp"),
        P(None, "tp"),
        P(),
    )
    out_specs = P(SP_TP, None)
    return jax.shard_map(
        shards, mesh=split, in_specs=in_specs, out_specs=out_specs, check_vma=False
    )
```

profile of v0, /device:TPU:1, one launch (start us, length us, event | category | flops | bytes accessed | tf_op | source)
XLA Modules:
  0.0 273.3 jit_solution(8756651230453433856)
XLA Ops:
  6.5 0.8 slice.239
  7.4 4.5 %collective-permute-start.1 = (bf16[3,128]{1,0:T(4,128)(2,1)S(1)}, bf16[3,128]{1,0:T(4,128)(2,1)S(1)}, u32[]{:S(2)}, u32[]{:S(2)}) collective-permute-start(bf16[3,128]{1,0:T(4,128)(2,1)S(1)} %slice.239), channel_id=1, source_target_pairs={{0,4},{4,8},{8,12},{12,16},{16,20},{20,24},{24,28},{28,32},{32,36}... | collective-permute-start | bytes 2312 | tf_op jit(solution)/shard_map/ppermute | solution.py:36
  11.9 0.7 slice.230
  12.6 1.9 collective-permute-start
  14.5 0.8 bitcast_convert_fusion.7
  15.3 1.4 slice_convert_fusion.3
  16.8 0.8 fusion.171
  17.6 1.1 reduce-window.6
  19.0 0.7 exponential_bitcast_fusion
  19.8 2.0 all_gather.29
  21.8 8.0 %all_gather.30 = bf16[4,1,8]{2,1,0:T(2,128)(2,1)S(1)} all-gather(bf16[1,1,8]{2,1,0:T(2,128)(2,1)S(1)} %multiply_convert_fusion.8), channel_id=1, replica_groups=mesh['sp_0'=8,'sp_1'=4,'sp_2'=2,'tp'=4] {'sp_1'}, dimensions={0}, use_global_device_ids=true | all-gather | bytes 80 | tf_op jit(solution)/shard_map/all_gather | solution.py:51
  29.8 0.6 fusion.165
  30.7 0.6 exponential_bitcast_fusion.1
  31.4 0.8 fusion.175
  32.2 0.6 fusion.154
  32.8 0.5 fusion.164
  33.3 0.6 copy.71
  34.0 0.9 maximum_convert_fusion.3
  35.4 0.6 fusion.53
  36.0 1.3 copy.70
  37.4 1.6 reshape.588
  38.9 1.8 broadcast_multiply_fusion
  41.1 5.7 %while.13 = (s32[]{:T(128)}, f32[1,8,64,128]{3,2,1,0:T(8,128)S(1)}, bf16[4,1,8,64,128]{4,3,2,1,0:T(8,128)(2,1)}, f32[4,1,8]{2,1,0:T(1,128)}, f32[4,1,8,64,128]{4,3,2,1,0:T(8,128)S(1)}, /*index=5*/s32[]{:T(128)}, s32[]{:T(128)}) while((s32[]{:T(128)}, f32[1,8,64,128]{3,2,1,0:T(8,128)S(1)}, bf16[4,1,8,64,128]{4,3,2,1,0:T(8,128)(2,1)}, ...), condition=%wide.region_2.3_spmd.clone, body=%wide.region_1.2_spmd.clone.sunk | while | flops 262147 | bytes 1179852 | solution.py:201
  41.1 0.6 fusion.186
  41.7 0.7 bitcast_dynamic-update-slice_fusion.2
  42.5 0.6 fusion.186
  43.1 0.7 bitcast_dynamic-update-slice_fusion.2
  43.9 0.6 fusion.186
  44.5 0.7 bitcast_dynamic-update-slice_fusion.2
  45.3 0.6 fusion.186
  45.9 0.7 bitcast_dynamic-update-slice_fusion.2
  46.8 4.1 %all-gather = bf16[2,8,64,128]{3,2,1,0:T(8,128)(2,1)S(1)} all-gather(bf16[1,8,64,128]{3,2,1,0:T(8,128)(2,1)S(1)} %convert_element_type.491), channel_id=2, replica_groups=mesh['sp_0'=8,'sp_1'=4,'sp_2'=2,'tp'=4] {'sp_2'}, dimensions={0}, use_global_device_ids=true | all-gather | bytes 393216 | tf_op jit(solution)/shard_map/all_gather | solution.py:51
  50.9 0.7 fusion.107
  51.6 9.9 %all_gather.34 = bf16[4,1,8,64,128]{4,3,2,1,0:T(8,128)(2,1)S(1)} all-gather(bf16[1,1,8,64,128]{4,3,2,1,0:T(8,128)(2,1)S(1)} %fusion.107), channel_id=1, replica_groups=mesh['sp_0'=8,'sp_1'=4,'sp_2'=2,'tp'=4] {'sp_1'}, dimensions={0}, use_global_device_ids=true | all-gather | bytes 655360 | tf_op jit(solution)/shard_map/all_gather | solution.py:51
  61.5 0.8 copy-done.5
  62.4 1.5 fusion.106
  64.0 1.7 pad_maximum_fusion
  65.7 3.9 %collective-permute-start.2 = (bf16[3,128]{1,0:T(4,128)(2,1)S(1)}, bf16[3,128]{1,0:T(4,128)(2,1)S(1)}, u32[]{:S(2)}, u32[]{:S(2)}) collective-permute-start(bf16[3,128]{1,0:T(4,128)(2,1)S(1)} %slice.248), channel_id=1, source_target_pairs={{0,4},{4,8},{8,12},{12,16},{16,20},{20,24},{24,28},{28,32},{32,36}... | collective-permute-start | bytes 2312 | tf_op jit(solution)/shard_map/ppermute | solution.py:36
  69.7 14.4 %all_gather.31 = bf16[8,1,8]{2,1,0:T(2,128)(2,1)S(1)} all-gather(bf16[1,1,8]{2,1,0:T(2,128)(2,1)S(1)} %multiply_convert_fusion.7), channel_id=1, replica_groups=mesh['sp_0'=8,'sp_1'=4,'sp_2'=2,'tp'=4] {'sp_0'}, dimensions={0}, use_global_device_ids=true | all-gather | bytes 144 | tf_op jit(solution)/shard_map/all_gather | solution.py:51
  84.1 0.6 iota_compare_fusion
  84.7 0.6 fusion.163
  85.3 0.6 fusion.161
  85.9 0.7 copy.74
  87.3 2.1 fusion.28
  89.4 1.4 fusion.35
  90.9 1.7 copy.82
  92.5 8.7 %all-gather.4.cloned.1.call-done = bf16[8,1,8,64,128]{4,3,2,1,0:T(8,128)(2,1)} async-done(((bf16[1,1,8,64,128]{4,3,2,1,0:T(8,128)(2,1)}), bf16[8,1,8,64,128]{4,3,2,1,0:T(8,128)(2,1)}) %all-gather.4.cloned.1.call-update) | async-done | bytes 1048592 | tf_op jit(solution)/shard_map/all_gather | solution.py:51
  101.2 3.6 %fusion.33 = f32[512,1,8,64]{0,3,2,1:T(8,128)} fusion(f32[512,1,8,64]{0,1,3,2:T(1,128)} %bitcast.234, f32[512,1,8,64]{0,3,2,1:T(8,128)S(1)} %bitcast.225, f32[8]{0:T(128)} %param.33, f32[512,8]{0,1:T(8,128)} %get-tuple-element.91, bf16[8,1,8,64,128]{4,3,2,1,0:T(8,128)(2,1)} %all-gather.4.cloned.1.call-done, ...), kind=kOutput, calls=%fused_computation.41 | convolution fusion | flops 71892992 | bytes 5128750 | tf_op jit(solution)/shard_map/tgn,ghpn->tghp/dot_general | solution.py:210
  104.9 1.6 copy.87
  106.4 1.5 multiply_reduce_fusion.2
  107.9 2.5 convolution_convert_fusion
  110.4 25.8 %all_to_all.15 = bf16[4,128,2048]{2,1,0:T(8,128)(2,1)S(1)} all-to-all(bf16[4,128,2048]{2,1,0:T(8,128)(2,1)S(1)} %bitcast.229), channel_id=1, replica_groups=mesh['sp_0'=8,'sp_1'=4,'sp_2'=2,'tp'=4] {'tp'}, dimensions={0} | all-to-all | bytes 4194304 | tf_op jit(solution)/shard_map/all_to_all | solution.py:73
  137.5 1.6 broadcast_in_dim.20
  139.1 4.6 %all-to-all-start.1 = ((bf16[4,128,2048]{2,1,0:T(8,128)(2,1)}), bf16[4,128,2048]{2,1,0:T(8,128)(2,1)}, u32[]{:S(2)}, u32[]{:S(2)}) async-start(bf16[4,128,2048]{2,1,0:T(8,128)(2,1)} %broadcast_in_dim.20), calls=%async_computation.1 | async-start | bytes 4194304 | tf_op jit(solution)/shard_map/all_to_all | solution.py:85
  143.9 19.8 %all-to-all-done.1 = bf16[4,128,2048]{2,1,0:T(8,128)(2,1)} async-done(((bf16[4,128,2048]{2,1,0:T(8,128)(2,1)}), bf16[4,128,2048]{2,1,0:T(8,128)(2,1)}, u32[]{:S(2)}, u32[]{:S(2)}) %all-to-all-start.1) | async-done | bytes 2097184 | tf_op jit(solution)/shard_map/all_to_all | solution.py:85
  163.7 44.6 %all-gather.6.cloned.1.call-done = bf16[2048,4224]{1,0:T(8,128)(2,1)} async-done(((bf16[32,4224]{1,0:T(8,128)(2,1)}), bf16[2048,4224]{1,0:T(8,128)(2,1)}) %all-gather.6.cloned.1.call-update) | async-done | bytes 17301520 | tf_op jit(solution)/shard_map/all_gather | solution.py:25
  208.2 6.7 %fusion.7 = bf16[512,1408]{1,0:T(8,128)(2,1)S(1)} fusion(bf16[512,2048]{1,0:T(8,128)(2,1)} %bitcast.67, bf16[2048,4224]{1,0:T(8,128)(2,1)} %all-gather.6.cloned.1.call-done), kind=kOutput, calls=%fused_computation.12 | convolution fusion | flops 2953510912 | bytes 9306112 | tf_op jit(solution)/shard_map/dot_general | solution.py:232
  214.9 2.0 collective-permute-start.3
  217.0 6.7 %fusion.10 = bf16[512,1408]{1,0:T(8,128)(2,1)S(1)} fusion(bf16[512,2048]{1,0:T(8,128)(2,1)} %bitcast.67, bf16[2048,4224]{1,0:T(8,128)(2,1)} %all-gather.6.cloned.1.call-done), kind=kOutput, calls=%fused_computation.13 | convolution fusion | flops 2953510912 | bytes 9306112 | tf_op jit(solution)/shard_map/dot_general | solution.py:233
  223.7 2.2 collective-permute-start.4
  226.1 0.6 collective-permute-done.4
  227.0 7.6 %fusion.13 = bf16[512,2048]{1,0:T(8,128)(2,1)S(1)} fusion(bf16[2048,4224]{1,0:T(8,128)(2,1)} %all-gather.6.cloned.1.call-done, f32[514,1408]{1,0:T(8,128)S(1)} %maximum_convert_fusion.1, f32[514,1408]{1,0:T(8,128)S(1)} %maximum_convert_fusion, f32[1408]{0:T(1024)S(1)} %get-tuple-element.77, f32[1408]{0:T(1024)S(1)} %get-tuple-element.78, ...), kind=kOutput, calls=%fused_computation.15 | convolution fusion | flops 2965372928 | bytes 25214976 | tf_op jit(solution)/shard_map/dot_general | solution.py:243
  234.7 29.8 %all_to_all.16 = bf16[4,128,2048]{2,1,0:T(8,128)(2,1)S(1)} all-to-all(bf16[4,128,2048]{2,1,0:T(8,128)(2,1)S(1)} %bitcast.228), channel_id=1, replica_groups=mesh['sp_0'=8,'sp_1'=4,'sp_2'=2,'tp'=4] {'tp'}, dimensions={0} | all-to-all | bytes 4194304 | tf_op jit(solution)/shard_map/all_to_all | solution.py:73
  265.4 1.1 multiply_convert_fusion
  (101 shorter events, 5.6 us)
Async XLA Ops:
  6.5 101.4 %copy-start = (bf16[512,2048]{1,0:T(8,128)(2,1)S(1)}, bf16[512,2048]{1,0:T(8,128)(2,1)}, u32[]{:S(2)}) copy-start(bf16[512,2048]{1,0:T(8,128)(2,1)} %param.38) | copy-start | bytes 6291460
  6.5 28.6 %copy-start.9 = (bf16[512,512]{1,0:T(8,128)(2,1)S(1)}, bf16[512,512]{1,0:T(8,128)(2,1)}, u32[]{:S(2)}) copy-start(bf16[512,512]{1,0:T(8,128)(2,1)} %param.26) | copy-start | bytes 1572868
  6.5 94.7 %all-gather.4.cloned.1.call-start = ((), (), s32[]{:S(2)}) async-start(), calls=%async_computation.3 | async-start | bytes 1179648 | tf_op jit(solution)/shard_map/all_gather | solution.py:51
  7.4 26.7 %collective-permute-start.1 = (bf16[3,128]{1,0:T(4,128)(2,1)S(1)}, bf16[3,128]{1,0:T(4,128)(2,1)S(1)}, u32[]{:S(2)}, u32[]{:S(2)}) collective-permute-start(bf16[3,128]{1,0:T(4,128)(2,1)S(1)} %slice.239), channel_id=1, source_target_pairs={{0,4},{4,8},{8,12},{12,16},{16,20},{20,24},{24,28},{28,32},{32,36}... | collective-permute-start | bytes 2312 | tf_op jit(solution)/shard_map/ppermute | solution.py:36
  12.6 22.6 %collective-permute-start = (bf16[3,512]{1,0:T(4,128)(2,1)S(1)}, bf16[3,512]{1,0:T(4,128)(2,1)S(1)}, u32[]{:S(2)}, u32[]{:S(2)}) collective-permute-start(bf16[3,512]{1,0:T(4,128)(2,1)S(1)} %slice.230), channel_id=1, source_target_pairs={{0,4},{4,8},{8,12},{12,16},{16,20},{20,24},{24,28},{28,32},{32,36}... | collective-permute-start | bytes 9224 | tf_op jit(solution)/shard_map/ppermute | solution.py:36
  29.8 5.5 %copy-start.11 = (bf16[4,1,8]{2,1,0:T(2,128)(2,1)}, bf16[4,1,8]{2,1,0:T(2,128)(2,1)S(1)}, u32[]{:S(2)}) copy-start(bf16[4,1,8]{2,1,0:T(2,128)(2,1)S(1)} %all_gather.30) | copy-start | bytes 196
  30.7 0.7 copy-start.3
  34.0 1.4 copy-start.15
  34.0 1.4 copy-start.16
  34.0 1.4 copy-start.17
  34.0 1.4 copy-start.18
  41.0 9.9 %copy-start.23 = (f32[8]{0:T(128)S(1)}, f32[8]{0:T(128)}, u32[]{:S(2)}) copy-start(f32[8]{0:T(128)} %get-tuple-element.117) | copy-start | bytes 100
  41.1 21.3 %copy-start.22 = (f32[8]{0:T(128)S(1)}, f32[8]{0:T(128)}, u32[]{:S(2)}) copy-start(f32[8]{0:T(128)} %get-tuple-element.113) | copy-start | bytes 100
  46.7 19.0 %copy-start.10 = (bf16[512,128]{1,0:T(8,128)(2,1)S(1)}, bf16[512,128]{1,0:T(8,128)(2,1)}, u32[]{:S(2)}) copy-start(bf16[512,128]{1,0:T(8,128)(2,1)} %param.28) | copy-start | bytes 393220
  46.7 22.9 %copy-start.12 = (bf16[4,1,8]{2,1,0:T(2,128)(2,1)S(1)}, bf16[4,1,8]{2,1,0:T(2,128)(2,1)}, u32[]{:S(2)}) copy-start(bf16[4,1,8]{2,1,0:T(2,128)(2,1)} %copy-done.11) | copy-start | bytes 196
  46.7 38.5 %copy-start.21 = (bf16[4,128]{1,0:T(4,128)(2,1)S(1)}, bf16[4,128]{1,0:T(4,128)(2,1)}, u32[]{:S(2)}) copy-start(bf16[4,128]{1,0:T(4,128)(2,1)} %param.36) | copy-start | bytes 3076
  46.8 39.1 %copy-start.4 = (f32[4,128,1,8]{3,2,1,0:T(1,128)S(1)}, f32[4,128,1,8]{3,2,1,0:T(1,128)}, u32[]{:S(2)}) copy-start(f32[4,128,1,8]{3,2,1,0:T(1,128)} %copy-done.3) | copy-start | bytes 49156
  46.8 39.8 %copy-start.6 = (f32[4,128,8]{2,1,0:T(8,128)S(1)}, f32[4,128,8]{2,1,0:T(8,128)}, u32[]{:S(2)}) copy-start(f32[4,128,8]{2,1,0:T(8,128)} %get-tuple-element.95) | copy-start | bytes 49156
  50.9 36.4 %copy-start.7 = (bf16[2,8,64,128]{3,2,1,0:T(8,128)(2,1)}, bf16[2,8,64,128]{3,2,1,0:T(8,128)(2,1)S(1)}, u32[]{:S(2)}) copy-start(bf16[2,8,64,128]{3,2,1,0:T(8,128)(2,1)S(1)} %all-gather) | copy-start | bytes 786436
  61.5 0.8 copy-start.5
  63.9 144.3 %all-gather.6.cloned.1.call-start = ((), (), s32[]{:S(2)}) async-start(), calls=%async_computation.4 | async-start | bytes 17571840 | tf_op jit(solution)/shard_map/all_gather | solution.py:25
  65.7 21.0 %collective-permute-start.2 = (bf16[3,128]{1,0:T(4,128)(2,1)S(1)}, bf16[3,128]{1,0:T(4,128)(2,1)S(1)}, u32[]{:S(2)}, u32[]{:S(2)}) collective-permute-start(bf16[3,128]{1,0:T(4,128)(2,1)S(1)} %slice.248), channel_id=1, source_target_pairs={{0,4},{4,8},{8,12},{12,16},{16,20},{20,24},{24,28},{28,32},{32,36}... | collective-permute-start | bytes 2312 | tf_op jit(solution)/shard_map/ppermute | solution.py:36
  89.4 11.8 %copy-start.2 = (f32[512,512]{0,1:T(8,128)S(1)}, f32[512,512]{0,1:T(8,128)}, u32[]{:S(2)}) copy-start(f32[512,512]{0,1:T(8,128)} %copy.70) | copy-start | bytes 3145732
  89.4 11.8 %copy-start.8 = (bf16[2,8,64,128]{3,2,1,0:T(8,128)(2,1)S(1)}, bf16[2,8,64,128]{3,2,1,0:T(8,128)(2,1)}, u32[]{:S(2)}) copy-start(bf16[2,8,64,128]{3,2,1,0:T(8,128)(2,1)} %copy-done.7) | copy-start | bytes 786436
  104.9 3.1 %copy-start.24 = (f32[512]{0:T(512)S(1)}, f32[512]{0:T(512)}, u32[]{:S(2)}) copy-start(f32[512]{0:T(512)} %param.37) | copy-start | bytes 6148
  110.4 26.2 %copy-start.1 = (bf16[128,2048]{1,0:T(8,128)(2,1)S(1)}, bf16[128,2048]{1,0:T(8,128)(2,1)}, u32[]{:S(2)}) copy-start(bf16[128,2048]{1,0:T(8,128)(2,1)} %param.24) | copy-start | bytes 1572868
  136.3 0.9 copy-start.19
  137.5 6.3 %copy-start.13 = (bf16[3,1408]{1,0:T(4,128)(2,1)S(1)}, bf16[3,1408]{1,0:T(4,128)(2,1)}, u32[]{:S(2)}) copy-start(bf16[3,1408]{1,0:T(4,128)(2,1)} %param.44) | copy-start | bytes 25348
  137.5 6.3 %copy-start.14 = (bf16[3,1408]{1,0:T(4,128)(2,1)S(1)}, bf16[3,1408]{1,0:T(4,128)(2,1)}, u32[]{:S(2)}) copy-start(bf16[3,1408]{1,0:T(4,128)(2,1)} %param.43) | copy-start | bytes 25348
  139.1 24.6 %all-to-all-start.1 = ((bf16[4,128,2048]{2,1,0:T(8,128)(2,1)}), bf16[4,128,2048]{2,1,0:T(8,128)(2,1)}, u32[]{:S(2)}, u32[]{:S(2)}) async-start(bf16[4,128,2048]{2,1,0:T(8,128)(2,1)} %broadcast_in_dim.20), calls=%async_computation.1 | async-start | bytes 4194304 | tf_op jit(solution)/shard_map/all_to_all | solution.py:85
  214.9 10.9 %collective-permute-start.3 = (bf16[2,1408]{1,0:T(2,128)(2,1)S(1)}, bf16[2,1408]{1,0:T(2,128)(2,1)S(1)}, u32[]{:S(2)}, u32[]{:S(2)}) collective-permute-start(bf16[2,1408]{1,0:T(2,128)(2,1)S(1)} %slice.351), channel_id=1, source_target_pairs={{0,4},{4,8},{8,12},{12,16},{16,20},{20,24},{24,28},{28,32},{32,36}... | collective-permute-start | bytes 16904 | tf_op jit(solution)/shard_map/ppermute | solution.py:36
  223.7 3.1 %collective-permute-start.4 = (bf16[2,1408]{1,0:T(2,128)(2,1)S(1)}, bf16[2,1408]{1,0:T(2,128)(2,1)S(1)}, u32[]{:S(2)}, u32[]{:S(2)}) collective-permute-start(bf16[2,1408]{1,0:T(2,128)(2,1)S(1)} %slice.356), channel_id=1, source_target_pairs={{0,4},{4,8},{8,12},{12,16},{16,20},{20,24},{24,28},{28,32},{32,36}... | collective-permute-start | bytes 16904 | tf_op jit(solution)/shard_map/ppermute | solution.py:36
  264.4 1.0 copy-start.20
Sparse Core Ops, SparseCore 0:
  64.0 37.1 all-gather.3
  103.9 104.2 all-gather.5
where the time goes:
time: 274 us; the launch traced here: 273 us
  blocking collectives  94 us (34%)
  waiting for transfers between devices  73.7 us (27%)
  matrix products  31.1 us (11%)
  other arithmetic  25.9 us (9%)
  starting transfers between devices  19.1 us (7%)
  local copies, waits for them, and re-layouts  15.4 us (6%)
  between operations  14 us (5%)
    all_to_all x2, blocking collectives, sent_and_summed(): lax.all_to_all(in_blocks(shard, dim, count), axis, 0, 0, tiled=True)  55.6 us
    all_gather x1, waiting for transfers between devices, gather_turned(): out, at, finished = (lax.all_gather(both, axis, axis=0, tiled=True), 0, [])  44.6 us
    all_gather x5, blocking collectives, entering(): lax.all_gather(part.astype(kind), axis)  38.4 us
    all_to_all x1, waiting for transfers between devices, sent_to_all(): return lax.all_to_all(copies, axis, split_axis=0, concat_axis=0, tiled=True)  19.8 us
    ppermute x5, starting transfers between devices, shifted(): return lax.ppermute(shard, axis, pairs)  14.5 us
    all_gather x1, waiting for transfers between devices, entering(): lax.all_gather(part.astype(kind), axis)  8.67 us
    dot_general x1, matrix products, shards(): jnp.dot(hidden, down_whole, preferred_element_type=jnp.float32)  7.63 us
    dot_general x1, matrix products, shards(): up_sum = jnp.dot(normed_all, up_whole, preferred_element_type=jnp.float32)  6.68 us
  transfers between devices with their start and end apart: 8, of which 4 were waited for; matrix products, arithmetic and copies ran while one was open for 15% of the time, Pallas kernels for 0%

commit v1 on v0

v1 whole, which is shorter than its diff:
```python
import jax
import jax.numpy as jnp
from jax import lax
from jax.experimental import pallas as pl
from jax.experimental.pallas import tpu as pltpu
from jax.sharding import Mesh
from jax.sharding import PartitionSpec as P

HEADS = 32
HEAD_DIM = 64
GROUPS = 4
STATE = 128
CONV = 4
FCONV = 3
BLOCK = 128
SP = ("sp_0", "sp_1", "sp_2")
SP_TP = ("sp_0", "sp_1", "sp_2", "tp")

EPSILON = 1e-05
ALPHA = 2.0**0.25
F32 = jnp.float32
BF16 = jnp.bfloat16
NEG = -1e30

ROWS = 512
CH = 512
NH = 8
QUARTER = 128
D = 2048
HALF = 1024
FFL = 1408

VMEM = pl.BlockSpec(memory_space=pltpu.VMEM)
SMEM = pl.BlockSpec(memory_space=pltpu.SMEM)


def dot(a, b):
    return jnp.dot(a, b, preferred_element_type=F32)


def dot_nt(a, b, precision=None):
    return lax.dot_general(
        a, b, (((1,), (1,)), ((), ())), precision=precision, preferred_element_type=F32
    )


def silu(v):
    return v / (1.0 + jnp.exp(-v))


def lane_pairs(column_of, rows):
    low = lax.broadcasted_iota(jnp.int32, (rows, 128), 1) < HEAD_DIM
    slabs = []
    for q in range(NH // 2):
        first = jnp.broadcast_to(column_of[:, 2 * q : 2 * q + 1], (rows, 128))
        second = jnp.broadcast_to(column_of[:, 2 * q + 1 : 2 * q + 2], (rows, 128))
        slabs.append(jnp.where(low, first, second))
    return slabs


def local_kernel(
    x_ref, b_ref, c_ref, rim_ref, xt_ref, bt_ref, ct_ref, delta_ref, extra_ref, head_ref,
    y_ref, cact_ref, grow_ref, msg_ref,
    xpad, bpad, cpad,
):
    xpad[0:8, :] = rim_ref[:, 0:CH].astype(F32)
    bpad[0:8, :] = rim_ref[:, CH : CH + STATE].astype(F32)
    cpad[0:8, :] = rim_ref[:, CH + STATE : CH + 2 * STATE].astype(F32)
    xpad[8 : 8 + ROWS, :] = x_ref[...].astype(F32)
    bpad[8 : 8 + ROWS, :] = b_ref[...].astype(F32)
    cpad[8 : 8 + ROWS, :] = c_ref[...].astype(F32)

    def conv(pad, taps, start):
        total = None
        for k in range(CONV):
            term = taps[k : k + 1, :].astype(F32) * pad[pl.ds(start + 8 - CONV + 1 + k, BLOCK), :]
            total = term if total is None else total + term
        return silu(total)

    offset = head_ref[0:1, :]
    speed = head_ref[1:2, :]
    bypass = lane_pairs(head_ref[2:3, :], 1)
    row = lax.broadcasted_iota(jnp.int32, (BLOCK, BLOCK), 0)
    col = lax.broadcasted_iota(jnp.int32, (BLOCK, BLOCK), 1)
    causal = row >= col
    lower = jnp.where(causal, 1.0, 0.0).astype(F32)
    eye = jnp.where(
        lax.broadcasted_iota(jnp.int32, (NH, NH), 0) == lax.broadcasted_iota(jnp.int32, (NH, NH), 1),
        1.0,
        0.0,
    ).astype(F32)
    low = col < HEAD_DIM
    state = [jnp.zeros((STATE, 128), F32) for _ in range(NH // 2)]
    base = jnp.zeros((1, NH), F32)
    for i in range(ROWS // BLOCK):
        start = i * BLOCK
        rows = pl.ds(start, BLOCK)
        step_in = delta_ref[rows, :] + offset
        step = jnp.maximum(step_in, 0.0) + jnp.log1p(jnp.exp(-jnp.abs(step_in)))
        fading = extra_ref[rows, :] - speed * step
        cum = jnp.dot(lower, fading, precision=lax.Precision.HIGHEST, preferred_element_type=F32)
        cum_t = dot_nt(eye, cum, precision=lax.Precision.HIGHEST)
        last = cum[BLOCK - 1 : BLOCK, :]
        x_act = conv(xpad, xt_ref, start).astype(BF16).astype(F32)
        b_act = conv(bpad, bt_ref, start).astype(BF16)
        c_act = conv(cpad, ct_ref, start).astype(BF16)
        cact_ref[rows, :] = c_act
        grow_ref[rows, :] = jnp.exp(base + cum)
        affinity = dot_nt(c_act, b_act)
        b_turned = b_act.astype(F32).T.astype(BF16)
        steps = lane_pairs(step, BLOCK)
        to_end = lane_pairs(jnp.exp(last - cum), BLOCK)
        grown = lane_pairs(jnp.exp(cum), BLOCK)
        kept = lane_pairs(jnp.exp(last), 1)
        for q in range(NH // 2):
            cols = slice(q * 128, (q + 1) * 128)
            x_here = x_act[:, cols]
            scaled = x_here * steps[q]
            narrow = scaled.astype(BF16)
            within = []
            for h in (2 * q, 2 * q + 1):
                between = cum[:, h : h + 1] - cum_t[h : h + 1, :]
                lag = jnp.exp(jnp.where(causal, between, NEG))
                within.append(dot((affinity * lag).astype(BF16), narrow))
            total = jnp.where(low, within[0], within[1]) + bypass[q] * x_here
            if i > 0:
                total = total + dot(c_act, state[q].astype(BF16)) * grown[q]
            y_ref[rows, cols] = total
            fresh = dot(b_turned, (scaled * to_end[q]).astype(BF16))
            state[q] = fresh if i == 0 else state[q] * kept[q] + fresh
        base = base + last
    totals = lane_pairs(base, 1)
    for q in range(NH // 2):
        block = slice(q * 16, (q + 1) * 16)
        msg_ref[block, 0:8, :] = state[q].reshape(16, 8, 128).astype(BF16)
        left = totals[q]
        parts = []
        for _ in range(3):
            part = left.astype(BF16)
            parts.append(part.astype(F32))
            left = left - part.astype(F32)
        line = lax.broadcasted_iota(jnp.int32, (8, 128), 0)
        packed = jnp.where(line == 0, parts[0], jnp.where(line == 1, parts[1], parts[2]))
        packed = jnp.where(line < 3, packed, 0.0).astype(BF16)
        msg_ref[block, 8:16, :] = jnp.broadcast_to(packed[None], (16, 8, 128))


def run_local(x, b, c, rim, xt, bt, ct, delta, extra, heads):
    return pl.pallas_call(
        local_kernel,
        out_shape=(
            jax.ShapeDtypeStruct((ROWS, CH), F32),
            jax.ShapeDtypeStruct((ROWS, STATE), BF16),
            jax.ShapeDtypeStruct((ROWS, NH), F32),
            jax.ShapeDtypeStruct((64, 16, 128), BF16),
        ),
        in_specs=[VMEM] * 10,
        out_specs=(VMEM,) * 4,
        scratch_shapes=[
            pltpu.VMEM((ROWS + 8, CH), F32),
            pltpu.VMEM((ROWS + 8, STATE), F32),
            pltpu.VMEM((ROWS + 8, STATE), F32),
        ],
        name="local_mixer",
    )(x, b, c, rim, xt, bt, ct, delta, extra, heads)


def prefix_kernel(in_ref, out_ref):
    entering = jnp.zeros((8, 128), F32)
    for j in range(64):
        out_ref[j] = entering.astype(BF16)
        piece = in_ref[j].astype(F32)
        total = piece[8:9, :] + piece[9:10, :] + piece[10:11, :]
        entering = entering * jnp.exp(total) + piece[0:8, :]


def run_prefix(received):
    return pl.pallas_call(
        prefix_kernel,
        out_shape=jax.ShapeDtypeStruct((64, 8, 128), BF16),
        in_specs=[VMEM],
        out_specs=VMEM,
        name="state_prefix",
    )(received)


def project_kernel(
    place_ref, y_ref, cact_ref, grow_ref, in_ref, valve_ref, scale_ref, w_ref,
    send_l, send_r, keep_l, keep_r, norm,
):
    for i in range(ROWS // BLOCK):
        rows = pl.ds(i * BLOCK, BLOCK)
        grown = lane_pairs(grow_ref[rows, :], BLOCK)
        c_act = cact_ref[rows, :]
        gated = []
        square = jnp.zeros((BLOCK, 1), F32)
        for q in range(NH // 2):
            cols = slice(q * 128, (q + 1) * 128)
            entering = in_ref[q * 16 : (q + 1) * 16].astype(F32).reshape(STATE, 128).astype(BF16)
            y = y_ref[rows, cols] + dot(c_act, entering) * grown[q]
            y = y * silu(valve_ref[rows, cols].astype(F32))
            gated.append(y)
            square = square + jnp.sum(y * y, axis=-1, keepdims=True)
        factor = lax.rsqrt(square * (1.0 / CH) + EPSILON)
        for q in range(NH // 2):
            cols = slice(q * 128, (q + 1) * 128)
            norm[rows, cols] = (gated[q] * factor * scale_ref[0:1, cols]).astype(BF16)

    def rows_of(k):
        return norm[pl.ds(pl.multiple_of(place_ref[k] * QUARTER, QUARTER), QUARTER), :]

    own, near, far, across = (rows_of(k) for k in range(4))
    left = w_ref[:, 0:HALF]
    right = w_ref[:, HALF:D]
    send_l[...] = dot(jnp.concatenate([near, across], axis=0), left).astype(BF16)
    send_r[...] = dot(jnp.concatenate([far, across], axis=0), right).astype(BF16)
    keep_l[...] = dot(jnp.concatenate([own, far], axis=0), left)
    keep_r[...] = dot(jnp.concatenate([own, near], axis=0), right)


def run_project(place, y, cact, grow, entering, valve, scale, w):
    return pl.pallas_call(
        project_kernel,
        out_shape=(
            jax.ShapeDtypeStruct((2 * QUARTER, HALF), BF16),
            jax.ShapeDtypeStruct((2 * QUARTER, HALF), BF16),
            jax.ShapeDtypeStruct((2 * QUARTER, HALF), F32),
            jax.ShapeDtypeStruct((2 * QUARTER, HALF), F32),
        ),
        in_specs=[SMEM] + [VMEM] * 7,
        out_specs=(VMEM,) * 4,
        scratch_shapes=[pltpu.VMEM((ROWS, CH), BF16)],
        name="gate_project",
    )(place, y, cact, grow, entering, valve, scale, w)


def normed_halves(values_l, values_r, scale_ref):
    mean = (
        jnp.sum(values_l, axis=-1, keepdims=True) + jnp.sum(values_r, axis=-1, keepdims=True)
    ) * (1.0 / D)
    left = values_l - mean
    right = values_r - mean
    spread = (
        jnp.sum(left * left, axis=-1, keepdims=True)
        + jnp.sum(right * right, axis=-1, keepdims=True)
    ) * (1.0 / D)
    factor = lax.rsqrt(spread + EPSILON)
    return left * factor * scale_ref[0:1, 0:HALF], right * factor * scale_ref[0:1, HALF:D]


def first_norm_kernel(
    keep_l, keep_r, once_l, once_r, twice_l, twice_r, res_ref, scale_ref, out_l, out_r
):
    left = keep_l[...] + once_l[...].astype(F32) + twice_l[...].astype(F32)
    right = keep_r[...] + once_r[...].astype(F32) + twice_r[...].astype(F32)
    left = left + ALPHA * res_ref[:, 0:HALF].astype(F32)
    right = right + ALPHA * res_ref[:, HALF:D].astype(F32)
    left, right = normed_halves(left, right, scale_ref)
    out_l[...] = left.astype(BF16)
    out_r[...] = right.astype(BF16)


def last_norm_kernel(
    keep_l, keep_r, once_l, once_r, twice_l, twice_r, res_l, res_r, scale_ref, out_ref
):
    left = keep_l[...] + once_l[...].astype(F32) + twice_l[...].astype(F32)
    right = keep_r[...] + once_r[...].astype(F32) + twice_r[...].astype(F32)
    left = left + ALPHA * res_l[...].astype(F32)
    right = right + ALPHA * res_r[...].astype(F32)
    left, right = normed_halves(left, right, scale_ref)
    out_ref[:, 0:HALF] = left.astype(BF16)
    out_ref[:, HALF:D] = right.astype(BF16)


TOP = pl.BlockSpec((QUARTER, HALF), lambda i: (0, 0))


def run_first_norm(keeps, onces, twices, residual, scale):
    return pl.pallas_call(
        first_norm_kernel,
        grid=(1,),
        out_shape=(jax.ShapeDtypeStruct((QUARTER, HALF), BF16),) * 2,
        in_specs=[TOP] * 6
        + [
            pl.BlockSpec((QUARTER, D), lambda i: (0, 0)),
            pl.BlockSpec((1, D), lambda i: (0, 0)),
        ],
        out_specs=(TOP, TOP),
        name="first_norm",
    )(*keeps, *onces, *twices, residual, scale)


def run_last_norm(keeps, onces, twices, own, scale):
    return pl.pallas_call(
        last_norm_kernel,
        grid=(1,),
        out_shape=jax.ShapeDtypeStruct((QUARTER, D), BF16),
        in_specs=[TOP] * 8 + [pl.BlockSpec((1, D), lambda i: (0, 0))],
        out_specs=pl.BlockSpec((QUARTER, D), lambda i: (0, 0)),
        name="last_norm",
    )(*keeps, *onces, *twices, *own, scale)


RIM = 16


def widen_kernel(
    place_ref, own_l, own_r, far_l, near_r, nf_l, nf_r, rim_ref, gate_w, up_w, gate_t, up_t,
    hid_ref, rows, gate_pad, up_pad,
):
    @pl.when(pl.program_id(0) == 0)
    def _():
        def at(k):
            return pl.ds(pl.multiple_of(RIM + place_ref[k] * QUARTER, RIM), QUARTER)

        left = slice(0, HALF)
        right = slice(HALF, D)
        rows[0:RIM, :] = rim_ref[...]
        rows[at(0), left] = own_l[...]
        rows[at(0), right] = own_r[...]
        rows[at(2), left] = far_l[...]
        rows[at(1), right] = near_r[...]
        rows[at(1), left] = nf_l[0:QUARTER, :]
        rows[at(3), left] = nf_l[QUARTER : 2 * QUARTER, :]
        rows[at(2), right] = nf_r[0:QUARTER, :]
        rows[at(3), right] = nf_r[QUARTER : 2 * QUARTER, :]

    both = dot(rows[...], jnp.concatenate([gate_w[...], up_w[...]], axis=1))
    both = both.astype(BF16).astype(F32)
    gate_pad[...] = both[:, 0:128]
    up_pad[...] = both[:, 128:256]

    def conv(pad, taps):
        total = None
        for k in range(FCONV):
            term = taps[k : k + 1, :].astype(F32) * pad[pl.ds(RIM - FCONV + 1 + k, ROWS), :]
            total = term if total is None else total + term
        return total

    hid_ref[...] = (silu(conv(gate_pad, gate_t)) * conv(up_pad, up_t)).astype(BF16)


def run_widen(place, pieces, rim, weights, gate_t, up_t):
    tiles = FFL // 128
    whole = lambda shape: pl.BlockSpec(shape, lambda j: (0, 0))
    return pl.pallas_call(
        widen_kernel,
        grid=(tiles,),
        out_shape=jax.ShapeDtypeStruct((ROWS, FFL), BF16),
        in_specs=[
            SMEM,
            whole((QUARTER, HALF)),
            whole((QUARTER, HALF)),
            whole((QUARTER, HALF)),
            whole((QUARTER, HALF)),
            whole((2 * QUARTER, HALF)),
            whole((2 * QUARTER, HALF)),
            whole((RIM, D)),
            pl.BlockSpec((D, 128), lambda j: (0, j)),
            pl.BlockSpec((D, 128), lambda j: (0, j + FFL // 128)),
            pl.BlockSpec((FCONV, 128), lambda j: (0, j)),
            pl.BlockSpec((FCONV, 128), lambda j: (0, j)),
        ],
        out_specs=pl.BlockSpec((ROWS, 128), lambda j: (0, j)),
        scratch_shapes=[
            pltpu.VMEM((ROWS + RIM, D), BF16),
            pltpu.VMEM((ROWS + RIM, 128), F32),
            pltpu.VMEM((ROWS + RIM, 128), F32),
        ],
        name="widen",
    )(place, *pieces, rim, weights, weights, gate_t, up_t)


NARROW = 512


def shrink_kernel(place_ref, hid_ref, w_ref, out_ref):
    half = pl.program_id(0) // (HALF // NARROW)

    def rows_of(k):
        return hid_ref[pl.ds(pl.multiple_of(place_ref[half, k] * QUARTER, QUARTER), QUARTER), :]

    lhs = jnp.concatenate([rows_of(0), rows_of(1)], axis=0)
    out_ref[...] = dot_nt(lhs, w_ref[...]).astype(out_ref.dtype)


def run_shrink(place, hidden, weights, kind, name):
    return pl.pallas_call(
        shrink_kernel,
        grid=(D // NARROW,),
        out_shape=jax.ShapeDtypeStruct((2 * QUARTER, D), kind),
        in_specs=[
            SMEM,
            pl.BlockSpec((ROWS, FFL), lambda j: (0, 0)),
            pl.BlockSpec((NARROW, FFL), lambda j: (j, 2)),
        ],
        out_specs=pl.BlockSpec((2 * QUARTER, NARROW), lambda j: (0, j)),
        name=name,
    )(place, hidden, weights)


NEAR = [(0, 1), (1, 0), (2, 3), (3, 2)]
FAR = [(0, 3), (3, 0), (1, 2), (2, 1)]


def with_near(part):
    return lax.ppermute(part, "tp", NEAR)


def with_far(part):
    return lax.ppermute(part, "tp", FAR)


def summed_halves(keeps, sends):
    once_l = with_near(sends[0])
    once_r = with_far(sends[1])
    on_l = (keeps[0][QUARTER:] + once_l[QUARTER:].astype(F32)).astype(BF16)
    on_r = (keeps[1][QUARTER:] + once_r[QUARTER:].astype(F32)).astype(BF16)
    return (once_l, once_r), (with_far(on_l), with_near(on_r))


def next_positions(shard):
    count = lax.axis_size(SP)
    return lax.ppermute(shard, SP, [(i, i + 1) for i in range(count - 1)])


def shards(
    incoming_residual_stream,
    result_valve,
    channel_feed_matrix,
    memory_feed_matrix,
    memory_query_matrix,
    unsoftened_deltas,
    delta_offset,
    channel_fading_speed,
    extra_log_fading,
    bypass_factor,
    channel_feed_kernel,
    memory_feed_kernel,
    memory_query_kernel,
    cluster_scaling_vector,
    mixer_result_matrix,
    initial_scaling_vector,
    valve_matrix,
    widen_matrix,
    shrink_matrix,
    valve_filter_kernel,
    widen_filter_kernel,
    latter_scaling_vector,
):
    own = lax.axis_index("tp").astype(jnp.int32)
    near = own ^ 1
    far = 3 - own
    across = own ^ 2
    place = jnp.stack([own, near, far, across])
    sent = jnp.stack([jnp.stack([near, across]), jnp.stack([far, across])])
    held = jnp.stack([jnp.stack([own, far]), jnp.stack([own, near])])

    weights = lax.all_gather(
        jnp.concatenate([valve_matrix, widen_matrix, shrink_matrix.T], axis=1), SP, tiled=True
    )

    rim = next_positions(
        jnp.concatenate(
            [
                channel_feed_matrix[ROWS - 8 :],
                memory_feed_matrix[ROWS - 8 :],
                memory_query_matrix[ROWS - 8 :],
            ],
            axis=1,
        )
    )
    heads = jnp.stack([delta_offset, channel_fading_speed, bypass_factor])
    y_local, c_act, grow, message = run_local(
        channel_feed_matrix,
        memory_feed_matrix,
        memory_query_matrix,
        rim,
        channel_feed_kernel,
        memory_feed_kernel,
        memory_query_kernel,
        unsoftened_deltas,
        extra_log_fading,
        heads,
    )
    received = lax.all_to_all(message, SP, 0, 0, tiled=True)
    entering = lax.all_to_all(run_prefix(received), SP, 0, 0, tiled=True)
    send_l, send_r, keep_l, keep_r = run_project(
        place,
        y_local,
        c_act,
        grow,
        entering,
        result_valve,
        cluster_scaling_vector.reshape(1, CH),
        mixer_result_matrix,
    )
    onces, twices = summed_halves((keep_l, keep_r), (send_l, send_r))
    own_l, own_r = run_first_norm(
        (keep_l, keep_r),
        onces,
        twices,
        incoming_residual_stream,
        initial_scaling_vector.reshape(1, D),
    )
    far_l = with_far(own_l)
    near_r = with_near(own_r)
    nf_l = with_near(jnp.concatenate([own_l, far_l], axis=0))
    nf_r = with_far(jnp.concatenate([own_r, near_r], axis=0))
    tail = slice(QUARTER - RIM, QUARTER)
    tail2 = slice(2 * QUARTER - RIM, 2 * QUARTER)
    is_last = own == 3
    near_last = near == 3
    far_last = far == 3
    end_l = jnp.where(
        is_last,
        own_l[tail],
        jnp.where(far_last, far_l[tail], jnp.where(near_last, nf_l[tail], nf_l[tail2])),
    )
    end_r = jnp.where(
        is_last,
        own_r[tail],
        jnp.where(near_last, near_r[tail], jnp.where(far_last, nf_r[tail], nf_r[tail2])),
    )
    rim_rows = next_positions(jnp.concatenate([end_l, end_r], axis=1))
    hidden = run_widen(
        place,
        (own_l, own_r, far_l, near_r, nf_l, nf_r),
        rim_rows,
        weights,
        valve_filter_kernel,
        widen_filter_kernel,
    )
    sends = run_shrink(sent, hidden, weights, BF16, "shrink_sent")
    keeps = run_shrink(held, hidden, weights, F32, "shrink_held")
    halves = lambda both: (both[:, :HALF], both[:, HALF:])
    keep_halves = halves(keeps)
    onces, twices = summed_halves(keep_halves, halves(sends))
    return run_last_norm(
        keep_halves, onces, twices, (own_l, own_r), latter_scaling_vector.reshape(1, D)
    )


def solution(mesh):
    split = Mesh(mesh.devices.reshape(8, 4, 2, mesh.shape["tp"]), ("sp_0", "sp_1", "sp_2", "tp"))
    in_specs = (
        P(SP_TP, None),
        P(SP, "tp"),
        P(SP, "tp"),
        P(SP, "tp"),
        P(SP, "tp"),
        P(SP, "tp"),
        P("tp"),
        P("tp"),
        P(SP, "tp"),
        P("tp"),
        P(None, "tp"),
        P(None, "tp"),
        P(None, "tp"),
        P("tp"),
        P("tp", None),
        P(),
        P(SP, "tp"),
        P(SP, "tp"),
        P("tp", SP),
        P(None, "tp"),
        P(None, "tp"),
        P(),
    )
    out_specs = P(SP_TP, None)
    return jax.shard_map(
        shards, mesh=split, in_specs=in_specs, out_specs=out_specs, check_vma=False
    )
```

time: 274 us -> 195 us (0.71)
  blocking collectives: 94 us -> 26.6 us
  Pallas kernels: 0 us -> 46.7 us
  matrix products: 31.1 us -> 0 us
  waiting for transfers between devices: 73.7 us -> 59.3 us
  other arithmetic: 25.9 us -> 13 us
  starting transfers between devices: 19.1 us -> 23.6 us
  local copies, waits for them, and re-layouts: 15.4 us -> 11.2 us
    all_gather x2 -> x1, waiting for transfers between devices: 53.3 us -> 0.01 us  [shards(): lax.all_gather(jnp.concatenate([valve_matrix, widen_matrix, shrink_matrix...]
    ppermute x5 -> x14, waiting for transfers between devices: 0.6 us -> 48.8 us  [the longest x6 26.2 us: with_near(): return lax.ppermute(part, 'tp', NEAR)]
    pallas_call x0 -> x8, Pallas kernels: none -> 46.7 us  [the longest x1 14.7 us: run_widen(): pl.pallas_call(widen_kernel, grid=(tiles,), out_shape=jax.ShapeDtypeStruc...]
    all_gather x5 -> x0, blocking collectives: 38.4 us -> none  [entering(): lax.all_gather(part.astype(kind), axis)]
    dot_general x9 -> x0, matrix products: 31.1 us -> none  [the longest x1 7.63 us: shards(): jnp.dot(hidden, down_whole, preferred_element_type=jnp.float32)]
    all_to_all x2 -> x1, blocking collectives: 55.6 us -> 26.6 us  [shards(): received = lax.all_to_all(message, SP, 0, 0, tiled=True)]
    all_to_all x1, waiting for transfers between devices: 19.8 us -> 10.4 us  [shards(): entering = lax.all_to_all(run_prefix(received), SP, 0, 0, tiled=True)]
    mul x7 -> x0, other arithmetic: 5.48 us -> none  [the longest x4 2.37 us: causal_conv(): tap_weights[tap_index].astype(jnp.float32)]
  transfers between devices with their start and end apart: 8 -> 16, of which waited for: 4 -> 11; matrix products, arithmetic and copies ran while one was open for 15% -> 8% of each run, Pallas kernels for 0% -> 12%
where the time goes in v1:
time: 195 us; the launch traced here: 194 us
  waiting for transfers between devices  59.3 us (30%)
  Pallas kernels  46.7 us (24%)
  blocking collectives  26.6 us (14%)
  starting transfers between devices  23.6 us (12%)
  between operations  13.6 us (7%)
  other arithmetic  13 us (7%)
  local copies, waits for them, and re-layouts  11.2 us (6%)
    all_to_all x1, blocking collectives, shards(): received = lax.all_to_all(message, SP, 0, 0, tiled=True)  26.6 us
    ppermute x6, waiting for transfers between devices, with_near(): return lax.ppermute(part, 'tp', NEAR)  26.2 us
    ppermute x6, waiting for transfers between devices, with_far(): return lax.ppermute(part, 'tp', FAR)  21.8 us
    pallas_call x1, Pallas kernels, run_widen(): pl.pallas_call(widen_kernel, grid=(tiles,), out_shape=jax.ShapeDtypeStruc...  14.7 us
    pallas_call x2, Pallas kernels, run_shrink(): pl.pallas_call(shrink_kernel, grid=(D // NARROW,), out_shape=jax.ShapeDty...  12.1 us
    all_to_all x1, waiting for transfers between devices, shards(): entering = lax.all_to_all(run_prefix(received), SP, 0, 0, tiled=True)  10.4 us
    ppermute x2, starting transfers between devices, next_positions(): return lax.ppermute(shard, SP, [(i, i + 1) for i in range(count - 1)])  9.68 us
    ppermute x6, starting transfers between devices, with_far(): return lax.ppermute(part, 'tp', FAR)  7.01 us
  transfers between devices with their start and end apart: 16, of which 11 were waited for; matrix products, arithmetic and copies ran while one was open for 8% of the time, Pallas kernels for 12%

profile of v1, /device:TPU:1, one launch (start us, length us, event | category | flops | bytes accessed | tf_op | source)
XLA Modules:
  0.0 193.9 jit_solution(16533499069116778203)
XLA Ops:
  6.5 1.7 pad_maximum_fusion.2
  8.3 0.0 all-gather.2.cloned.1.call-update
  8.3 0.7 slice.72
  9.0 0.7 slice.73
  9.7 0.7 slice.71
  10.4 4.5 %collective-permute-start = (bf16[8,768]{1,0:T(8,128)(2,1)S(1)}, bf16[8,768]{1,0:T(8,128)(2,1)S(1)}, u32[]{:S(2)}, u32[]{:S(2)}) collective-permute-start(bf16[8,768]{1,0:T(8,128)(2,1)S(1)} %pad_maximum_fusion.4), channel_id=1, source_target_pairs={{0,4},{4,8},{8,12},{12,16},{16,20},{20,24},{24,28},{28,32},{32,36}... | collective-permute-start | bytes 36872 | tf_op jit(solution)/shard_map/ppermute | solution.py:424
  14.8 1.3 pad_maximum_fusion.5.head_ref
  16.1 1.6 copy.23.delta_ref
  17.7 1.6 copy.24.extra_ref
  19.2 0.0 collective-permute-done.rim_ref
  19.2 0.6 copy-done.15
  19.8 6.2 %local_mixer.1 = (f32[512,512]{1,0:T(8,128)}, bf16[512,128]{1,0:T(8,128)(2,1)}, f32[512,8]{1,0:T(8,128)}, bf16[64,16,128]{2,1,0:T(8,128)(2,1)}) custom-call(bf16[512,512]{1,0:T(8,128)(2,1)} %x_ref.1, bf16[512,128]{1,0:T(8,128)(2,1)} %b_ref.1, bf16[512,128]{1,0:T(8,128)(2,1)} %c_ref.1, bf16[8,768]{1,0:T(8,128)(2,1)} %copy-done.15, bf16[4,512]{1,0:T(4,128)(2,1)} %xt_ref.1, ...), custom_call_target="tpu_custom_call" | custom-call | tf_op jit(solution)/shard_map/local_mixer/pallas_call | solution.py:149
  26.1 26.6 %all_to_all.10.in_ref = bf16[64,16,128]{2,1,0:T(8,128)(2,1)} all-to-all(bf16[64,16,128]{2,1,0:T(8,128)(2,1)} %get-tuple-element.18), channel_id=1, replica_groups=mesh['sp_0'=8,'sp_1'=4,'sp_2'=2,'tp'=4] {'sp_0','sp_1','sp_2'}, dimensions={0} | all-to-all | bytes 524288 | tf_op jit(solution)/shard_map/all_to_all | solution.py:486
  52.6 1.8 state_prefix.1
  54.4 5.2 %all-to-all-start.1 = ((bf16[64,8,128]{2,1,0:T(8,128)(2,1)}), bf16[64,8,128]{2,1,0:T(8,128)(2,1)S(1)}, u32[]{:S(2)}, u32[]{:S(2)}) async-start(bf16[64,8,128]{2,1,0:T(8,128)(2,1)} %state_prefix.1), calls=%async_computation.1 | async-start | bytes 262144 | tf_op jit(solution)/shard_map/all_to_all | solution.py:487
  59.6 0.7 pad_add_fusion.2.place_ref
  60.3 10.4 %all-to-all-done.1.in_ref = bf16[64,8,128]{2,1,0:T(8,128)(2,1)S(1)} async-done(((bf16[64,8,128]{2,1,0:T(8,128)(2,1)}), bf16[64,8,128]{2,1,0:T(8,128)(2,1)S(1)}, u32[]{:S(2)}, u32[]{:S(2)}) %all-to-all-start.1) | async-done | bytes 131104 | tf_op jit(solution)/shard_map/all_to_all | solution.py:487
  70.7 0.7 copy-done.9
  71.3 5.9 %gate_project.1 = (bf16[256,1024]{1,0:T(8,128)(2,1)}, bf16[256,1024]{1,0:T(8,128)(2,1)}, f32[256,1024]{1,0:T(8,128)}, f32[256,1024]{1,0:T(8,128)}) custom-call(s32[4]{0:T(128)} %pad_add_fusion.2.place_ref, f32[512,512]{1,0:T(8,128)} %get-tuple-element.15.y_ref, bf16[512,128]{1,0:T(8,128)(2,1)} %get-tuple-element.16.cact_ref, ...), custom_call_target="tpu_custom_call" | custom-call | tf_op jit(solution)/shard_map/gate_project/pallas_call | solution.py:222
  77.3 1.3 collective-permute-start.1
  78.5 1.9 collective-permute-start.2
  80.4 10.4 %collective-permute-done.1.once_l = bf16[256,1024]{1,0:T(8,128)(2,1)S(1)} collective-permute-done((bf16[256,1024]{1,0:T(8,128)(2,1)}, bf16[256,1024]{1,0:T(8,128)(2,1)S(1)}, u32[]{:S(2)}, u32[]{:S(2)}) %collective-permute-start.1) | collective-permute-done | bytes 524320 | tf_op jit(solution)/shard_map/ppermute | solution.py:407
  90.8 1.3 add_convert_fusion.1
  92.1 2.6 %collective-permute-start.3 = (bf16[128,1024]{1,0:T(8,128)(2,1)S(1)}, bf16[128,1024]{1,0:T(8,128)(2,1)S(1)}, u32[]{:S(2)}, u32[]{:S(2)}) collective-permute-start(bf16[128,1024]{1,0:T(8,128)(2,1)S(1)} %add_convert_fusion.1), channel_id=1, source_target_pairs={{0,3},{3,0},{1,2},{2,1},{4,7},{7,4},{5,6},{6,5},{8,11},{11,8},{9,1... | collective-permute-start | bytes 786440 | tf_op jit(solution)/shard_map/ppermute | solution.py:411
  94.7 1.3 add_convert_fusion
  96.0 0.1 collective-permute-start.4
  96.1 4.1 %collective-permute-done.3.twice_l = bf16[128,1024]{1,0:T(8,128)(2,1)S(1)} collective-permute-done((bf16[128,1024]{1,0:T(8,128)(2,1)S(1)}, bf16[128,1024]{1,0:T(8,128)(2,1)S(1)}, u32[]{:S(2)}, u32[]{:S(2)}) %collective-permute-start.3) | collective-permute-done | bytes 262176 | tf_op jit(solution)/shard_map/ppermute | solution.py:411
  100.3 2.5 %collective-permute-done.4.twice_r = bf16[128,1024]{1,0:T(8,128)(2,1)S(1)} collective-permute-done((bf16[128,1024]{1,0:T(8,128)(2,1)S(1)}, bf16[128,1024]{1,0:T(8,128)(2,1)S(1)}, u32[]{:S(2)}, u32[]{:S(2)}) %collective-permute-start.4) | collective-permute-done | bytes 262176 | tf_op jit(solution)/shard_map/ppermute | solution.py:407
  102.8 0.7 copy-done.13
  103.4 3.0 %first_norm.1 = (bf16[128,1024]{1,0:T(8,128)(2,1)}, bf16[128,1024]{1,0:T(8,128)(2,1)}) custom-call(f32[256,1024]{1,0:T(8,128)} %get-tuple-element.19.keep_l, f32[256,1024]{1,0:T(8,128)} %get-tuple-element.20.keep_r, bf16[256,1024]{1,0:T(8,128)(2,1)} %copy-done.5, bf16[256,1024]{1,0:T(8,128)(2,1)} %copy-done.6, bf16[128,1024]{1,0:T(8,128)(2,1)} %copy-done.10, ...), custom_call_target="tpu_custom_call" | custom-call | tf_op jit(solution)/shard_map/first_norm/pallas_call | solution.py:279
  106.5 0.2 collective-permute-start.5
  106.7 0.0 collective-permute-start.6
  106.7 7.0 %collective-permute-done.5.far_l = bf16[128,1024]{1,0:T(8,128)(2,1)S(1)} collective-permute-done((bf16[128,1024]{1,0:T(8,128)(2,1)}, bf16[128,1024]{1,0:T(8,128)(2,1)S(1)}, u32[]{:S(2)}, u32[]{:S(2)}) %collective-permute-start.5) | collective-permute-done | bytes 262176 | tf_op jit(solution)/shard_map/ppermute | solution.py:411
  113.8 1.1 pad_maximum_fusion
  114.9 0.1 collective-permute-start.7
  115.0 0.0 collective-permute-done.6.near_r
  115.0 1.1 pad_maximum_fusion.1
  116.1 0.3 collective-permute-start.8
  116.4 0.1 add_bitcast_fusion
  116.5 0.1 add_bitcast_fusion.1
  116.6 9.1 %collective-permute-done.7.nf_l = bf16[256,1024]{1,0:T(8,128)(2,1)S(1)} collective-permute-done((bf16[256,1024]{1,0:T(8,128)(2,1)S(1)}, bf16[256,1024]{1,0:T(8,128)(2,1)S(1)}, u32[]{:S(2)}, u32[]{:S(2)}) %collective-permute-start.7) | collective-permute-done | bytes 524320 | tf_op jit(solution)/shard_map/ppermute | solution.py:407
  125.6 0.8 fusion.5
  126.4 1.6 collective-permute-done.8.nf_r
  128.0 0.8 fusion.3
  128.8 5.2 %collective-permute-start.9 = (bf16[16,2048]{1,0:T(8,128)(2,1)S(1)}, bf16[16,2048]{1,0:T(8,128)(2,1)S(1)}, u32[]{:S(2)}, u32[]{:S(2)}) collective-permute-start(bf16[16,2048]{1,0:T(8,128)(2,1)S(1)} %pad_maximum_fusion.3), channel_id=1, source_target_pairs={{0,4},{4,8},{8,12},{12,16},{16,20},{20,24},{24,28},{28,32},{32,36}... | collective-permute-start | bytes 196616 | tf_op jit(solution)/shard_map/ppermute | solution.py:424
  134.0 0.6 pad_add_fusion.1.place_ref
  134.6 0.7 collective-permute-done.9.rim_ref
  135.4 0.6 copy-done.14
  136.0 14.7 %widen.1.hid_ref = bf16[512,1408]{1,0:T(8,128)(2,1)} custom-call(s32[4]{0:T(128)} %pad_add_fusion.2.place_ref, bf16[128,1024]{1,0:T(8,128)(2,1)} %get-tuple-element.23.own_l.res_l, bf16[128,1024]{1,0:T(8,128)(2,1)} %get-tuple-element.24.own_r.res_r, bf16[128,1024]{1,0:T(8,128)(2,1)} %copy-done.1, bf16[128,1024]{1,0:T(8,128)(2,1)} %copy-done.2, ...), custom_call_target="tpu_custom_call" | custom-call | tf_op jit(solution)/shard_map/widen/pallas_call | solution.py:346
  150.6 6.0 %shrink_sent.1 = bf16[256,2048]{1,0:T(8,128)(2,1)} custom-call(s32[2,2]{1,0:T(2,128)} %pad_add_fusion.1.place_ref, bf16[512,1408]{1,0:T(8,128)(2,1)} %widen.1.hid_ref, bf16[2048,4224]{1,0:T(8,128)(2,1)} %all-gather.2.cloned.1.call-done.gate_w.up_w.w_ref), custom_call_target="tpu_custom_call" | custom-call | tf_op jit(solution)/shard_map/shrink_sent/pallas_call | solution.py:388
  156.6 1.3 fusion.7
  157.9 0.3 collective-permute-start.11
  158.2 0.1 collective-permute-start.10
  158.3 0.6 pad_add_fusion.place_ref
  158.9 6.1 %shrink_held.1 = f32[256,2048]{1,0:T(8,128)} custom-call(s32[2,2]{1,0:T(2,128)} %pad_add_fusion.place_ref, bf16[512,1408]{1,0:T(8,128)(2,1)} %widen.1.hid_ref, bf16[2048,4224]{1,0:T(8,128)(2,1)} %all-gather.2.cloned.1.call-done.gate_w.up_w.w_ref), custom_call_target="tpu_custom_call" | custom-call | tf_op jit(solution)/shard_map/shrink_held/pallas_call | solution.py:388
  165.0 7.7 %collective-permute-done.11.once_r = bf16[256,1024]{1,0:T(8,128)(2,1)S(1)} collective-permute-done((bf16[256,1024]{1,0:T(8,128)(2,1)S(1)}, bf16[256,1024]{1,0:T(8,128)(2,1)S(1)}, u32[]{:S(2)}, u32[]{:S(2)}) %collective-permute-start.11) | collective-permute-done | bytes 524320 | tf_op jit(solution)/shard_map/ppermute | solution.py:411
  172.8 1.7 fusion
  174.5 0.1 collective-permute-start.13
  174.6 1.6 collective-permute-start.12
  176.2 1.5 fusion.6
  177.8 4.3 %collective-permute-done.13.twice_r = bf16[128,1024]{1,0:T(8,128)(2,1)S(1)} collective-permute-done((bf16[128,1024]{1,0:T(8,128)(2,1)S(1)}, bf16[128,1024]{1,0:T(8,128)(2,1)S(1)}, u32[]{:S(2)}, u32[]{:S(2)}) %collective-permute-start.13) | collective-permute-done | bytes 262176 | tf_op jit(solution)/shard_map/ppermute | solution.py:407
  182.1 1.3 collective-permute-done.12.twice_l
  183.4 0.7 copy-done.12
  184.1 3.0 %last_norm.1 = bf16[128,2048]{1,0:T(8,128)(2,1)} custom-call(f32[256,1024]{1,0:T(8,128)} %get-tuple-element.28.keep_l, f32[256,1024]{1,0:T(8,128)} %get-tuple-element.27.keep_r, bf16[256,1024]{1,0:T(8,128)(2,1)} %copy-done.4, bf16[256,1024]{1,0:T(8,128)(2,1)} %copy-done.3, bf16[128,1024]{1,0:T(8,128)(2,1)} %copy-done.12, bf16[128,1024]{1,0:T(8,128)(2,1)} %copy-done.11, ...), custom_call_target="tpu_custom_call" | custom-call | tf_op jit(solution)/shard_map/last_norm/pallas_call | solution.py:294
  (33 shorter events, 0.1 us)
Async XLA Ops:
  6.5 128.8 %all-gather.2.cloned.1.call-start = ((), (), s32[]{:S(2)}) async-start(), calls=%async_computation.2 | async-start | bytes 17571840 | tf_op jit(solution)/shard_map/all_gather | solution.py:459
  10.4 8.9 %collective-permute-start = (bf16[8,768]{1,0:T(8,128)(2,1)S(1)}, bf16[8,768]{1,0:T(8,128)(2,1)S(1)}, u32[]{:S(2)}, u32[]{:S(2)}) collective-permute-start(bf16[8,768]{1,0:T(8,128)(2,1)S(1)} %pad_maximum_fusion.4), channel_id=1, source_target_pairs={{0,4},{4,8},{8,12},{12,16},{16,20},{20,24},{24,28},{28,32},{32,36}... | collective-permute-start | bytes 36872 | tf_op jit(solution)/shard_map/ppermute | solution.py:424
  19.2 0.6 copy-start.15
  54.4 16.3 %all-to-all-start.1 = ((bf16[64,8,128]{2,1,0:T(8,128)(2,1)}), bf16[64,8,128]{2,1,0:T(8,128)(2,1)S(1)}, u32[]{:S(2)}, u32[]{:S(2)}) async-start(bf16[64,8,128]{2,1,0:T(8,128)(2,1)} %state_prefix.1), calls=%async_computation.1 | async-start | bytes 262144 | tf_op jit(solution)/shard_map/all_to_all | solution.py:487
  70.7 0.7 copy-start.9
  77.3 13.5 %collective-permute-start.1 = (bf16[256,1024]{1,0:T(8,128)(2,1)}, bf16[256,1024]{1,0:T(8,128)(2,1)S(1)}, u32[]{:S(2)}, u32[]{:S(2)}) collective-permute-start(bf16[256,1024]{1,0:T(8,128)(2,1)} %get-tuple-element.21), channel_id=1, source_target_pairs={{0,1},{1,0},{2,3},{3,2},{4,5},{5,4},{6,7},{7,6},{8,9},{9,8},{10,11... | collective-permute-start | bytes 1572872 | tf_op jit(solution)/shard_map/ppermute | solution.py:407
  78.5 16.2 %collective-permute-start.2 = (bf16[256,1024]{1,0:T(8,128)(2,1)}, bf16[256,1024]{1,0:T(8,128)(2,1)S(1)}, u32[]{:S(2)}, u32[]{:S(2)}) collective-permute-start(bf16[256,1024]{1,0:T(8,128)(2,1)} %get-tuple-element.22), channel_id=1, source_target_pairs={{0,3},{3,0},{1,2},{2,1},{4,7},{7,4},{5,6},{6,5},{8,11},{11,8},{9,1... | collective-permute-start | bytes 1572872 | tf_op jit(solution)/shard_map/ppermute | solution.py:411
  90.8 12.0 %copy-start.5 = (bf16[256,1024]{1,0:T(8,128)(2,1)}, bf16[256,1024]{1,0:T(8,128)(2,1)S(1)}, u32[]{:S(2)}) copy-start(bf16[256,1024]{1,0:T(8,128)(2,1)S(1)} %collective-permute-done.1.once_l) | copy-start | bytes 1572868
  92.1 8.2 %collective-permute-start.3 = (bf16[128,1024]{1,0:T(8,128)(2,1)S(1)}, bf16[128,1024]{1,0:T(8,128)(2,1)S(1)}, u32[]{:S(2)}, u32[]{:S(2)}) collective-permute-start(bf16[128,1024]{1,0:T(8,128)(2,1)S(1)} %add_convert_fusion.1), channel_id=1, source_target_pairs={{0,3},{3,0},{1,2},{2,1},{4,7},{7,4},{5,6},{6,5},{8,11},{11,8},{9,1... | collective-permute-start | bytes 786440 | tf_op jit(solution)/shard_map/ppermute | solution.py:411
  94.7 8.0 %copy-start.6 = (bf16[256,1024]{1,0:T(8,128)(2,1)}, bf16[256,1024]{1,0:T(8,128)(2,1)S(1)}, u32[]{:S(2)}) copy-start(bf16[256,1024]{1,0:T(8,128)(2,1)S(1)} %collective-permute-done.2.once_r) | copy-start | bytes 1572868
  96.0 6.7 %collective-permute-start.4 = (bf16[128,1024]{1,0:T(8,128)(2,1)S(1)}, bf16[128,1024]{1,0:T(8,128)(2,1)S(1)}, u32[]{:S(2)}, u32[]{:S(2)}) collective-permute-start(bf16[128,1024]{1,0:T(8,128)(2,1)S(1)} %add_convert_fusion), channel_id=1, source_target_pairs={{0,1},{1,0},{2,3},{3,2},{4,5},{5,4},{6,7},{7,6},{8,9},{9,8},{10,11... | collective-permute-start | bytes 786440 | tf_op jit(solution)/shard_map/ppermute | solution.py:407
  100.3 2.5 %copy-start.10 = (bf16[128,1024]{1,0:T(8,128)(2,1)}, bf16[128,1024]{1,0:T(8,128)(2,1)S(1)}, u32[]{:S(2)}) copy-start(bf16[128,1024]{1,0:T(8,128)(2,1)S(1)} %collective-permute-done.3.twice_l) | copy-start | bytes 786436
  102.7 0.7 copy-start.13
  106.5 7.3 %collective-permute-start.5 = (bf16[128,1024]{1,0:T(8,128)(2,1)}, bf16[128,1024]{1,0:T(8,128)(2,1)S(1)}, u32[]{:S(2)}, u32[]{:S(2)}) collective-permute-start(bf16[128,1024]{1,0:T(8,128)(2,1)} %get-tuple-element.23.own_l.res_l), channel_id=1, source_target_pairs={{0,3},{3,0},{1,2},{2,1},{4,7},{7,4},{5,6},{6,5},{8,11},{11,8},{9,1... | collective-permute-start | bytes 786440 | tf_op jit(solution)/shard_map/ppermute | solution.py:411
  106.7 8.3 %collective-permute-start.6 = (bf16[128,1024]{1,0:T(8,128)(2,1)}, bf16[128,1024]{1,0:T(8,128)(2,1)S(1)}, u32[]{:S(2)}, u32[]{:S(2)}) collective-permute-start(bf16[128,1024]{1,0:T(8,128)(2,1)} %get-tuple-element.24.own_r.res_r), channel_id=1, source_target_pairs={{0,1},{1,0},{2,3},{3,2},{4,5},{5,4},{6,7},{7,6},{8,9},{9,8},{10,11... | collective-permute-start | bytes 786440 | tf_op jit(solution)/shard_map/ppermute | solution.py:407
  113.8 21.6 %copy-start.1 = (bf16[128,1024]{1,0:T(8,128)(2,1)}, bf16[128,1024]{1,0:T(8,128)(2,1)S(1)}, u32[]{:S(2)}) copy-start(bf16[128,1024]{1,0:T(8,128)(2,1)S(1)} %collective-permute-done.5.far_l) | copy-start | bytes 786436
  114.9 10.8 %collective-permute-start.7 = (bf16[256,1024]{1,0:T(8,128)(2,1)S(1)}, bf16[256,1024]{1,0:T(8,128)(2,1)S(1)}, u32[]{:S(2)}, u32[]{:S(2)}) collective-permute-start(bf16[256,1024]{1,0:T(8,128)(2,1)S(1)} %pad_maximum_fusion), channel_id=1, source_target_pairs={{0,1},{1,0},{2,3},{3,2},{4,5},{5,4},{6,7},{7,6},{8,9},{9,8},{10,11... | collective-permute-start | bytes 1572872 | tf_op jit(solution)/shard_map/ppermute | solution.py:407
  115.0 20.4 %copy-start.2 = (bf16[128,1024]{1,0:T(8,128)(2,1)}, bf16[128,1024]{1,0:T(8,128)(2,1)S(1)}, u32[]{:S(2)}) copy-start(bf16[128,1024]{1,0:T(8,128)(2,1)S(1)} %collective-permute-done.6.near_r) | copy-start | bytes 786436
  116.1 12.0 %collective-permute-start.8 = (bf16[256,1024]{1,0:T(8,128)(2,1)S(1)}, bf16[256,1024]{1,0:T(8,128)(2,1)S(1)}, u32[]{:S(2)}, u32[]{:S(2)}) collective-permute-start(bf16[256,1024]{1,0:T(8,128)(2,1)S(1)} %pad_maximum_fusion.1), channel_id=1, source_target_pairs={{0,3},{3,0},{1,2},{2,1},{4,7},{7,4},{5,6},{6,5},{8,11},{11,8},{9,1... | collective-permute-start | bytes 1572872 | tf_op jit(solution)/shard_map/ppermute | solution.py:411
  125.6 9.7 %copy-start.7 = (bf16[256,1024]{1,0:T(8,128)(2,1)}, bf16[256,1024]{1,0:T(8,128)(2,1)S(1)}, u32[]{:S(2)}) copy-start(bf16[256,1024]{1,0:T(8,128)(2,1)S(1)} %collective-permute-done.7.nf_l) | copy-start | bytes 1572868
  128.0 7.3 %copy-start.8 = (bf16[256,1024]{1,0:T(8,128)(2,1)}, bf16[256,1024]{1,0:T(8,128)(2,1)S(1)}, u32[]{:S(2)}) copy-start(bf16[256,1024]{1,0:T(8,128)(2,1)S(1)} %collective-permute-done.8.nf_r) | copy-start | bytes 1572868
  128.8 6.5 %collective-permute-start.9 = (bf16[16,2048]{1,0:T(8,128)(2,1)S(1)}, bf16[16,2048]{1,0:T(8,128)(2,1)S(1)}, u32[]{:S(2)}, u32[]{:S(2)}) collective-permute-start(bf16[16,2048]{1,0:T(8,128)(2,1)S(1)} %pad_maximum_fusion.3), channel_id=1, source_target_pairs={{0,4},{4,8},{8,12},{12,16},{16,20},{20,24},{24,28},{28,32},{32,36}... | collective-permute-start | bytes 196616 | tf_op jit(solution)/shard_map/ppermute | solution.py:424
  135.3 0.6 copy-start.14
  157.9 14.9 %collective-permute-start.11 = (bf16[256,1024]{1,0:T(8,128)(2,1)S(1)}, bf16[256,1024]{1,0:T(8,128)(2,1)S(1)}, u32[]{:S(2)}, u32[]{:S(2)}) collective-permute-start(bf16[256,1024]{1,0:T(8,128)(2,1)S(1)} %get-tuple-element.29), channel_id=1, source_target_pairs={{0,3},{3,0},{1,2},{2,1},{4,7},{7,4},{5,6},{6,5},{8,11},{11,8},{9,1... | collective-permute-start | bytes 1572872 | tf_op jit(solution)/shard_map/ppermute | solution.py:411
  158.2 14.6 %collective-permute-start.10 = (bf16[256,1024]{1,0:T(8,128)(2,1)S(1)}, bf16[256,1024]{1,0:T(8,128)(2,1)S(1)}, u32[]{:S(2)}, u32[]{:S(2)}) collective-permute-start(bf16[256,1024]{1,0:T(8,128)(2,1)S(1)} %get-tuple-element.30), channel_id=1, source_target_pairs={{0,1},{1,0},{2,3},{3,2},{4,5},{5,4},{6,7},{7,6},{8,9},{9,8},{10,11... | collective-permute-start | bytes 1572872 | tf_op jit(solution)/shard_map/ppermute | solution.py:407
  165.0 11.2 %copy-start = (f32[256,2048]{1,0:T(8,128)S(1)}, f32[256,2048]{1,0:T(8,128)}, u32[]{:S(2)}) copy-start(f32[256,2048]{1,0:T(8,128)} %shrink_held.1) | copy-start | bytes 6291460
  172.8 5.0 %copy-start.3 = (bf16[256,1024]{1,0:T(8,128)(2,1)}, bf16[256,1024]{1,0:T(8,128)(2,1)S(1)}, u32[]{:S(2)}) copy-start(bf16[256,1024]{1,0:T(8,128)(2,1)S(1)} %collective-permute-done.11.once_r) | copy-start | bytes 1572868
  172.8 5.0 %copy-start.4 = (bf16[256,1024]{1,0:T(8,128)(2,1)}, bf16[256,1024]{1,0:T(8,128)(2,1)S(1)}, u32[]{:S(2)}) copy-start(bf16[256,1024]{1,0:T(8,128)(2,1)S(1)} %collective-permute-done.10.once_l) | copy-start | bytes 1572868
  174.5 7.6 %collective-permute-start.13 = (bf16[128,1024]{1,0:T(8,128)(2,1)S(1)}, bf16[128,1024]{1,0:T(8,128)(2,1)S(1)}, u32[]{:S(2)}, u32[]{:S(2)}) collective-permute-start(bf16[128,1024]{1,0:T(8,128)(2,1)S(1)} %get-tuple-element.25), channel_id=1, source_target_pairs={{0,1},{1,0},{2,3},{3,2},{4,5},{5,4},{6,7},{7,6},{8,9},{9,8},{10,11... | collective-permute-start | bytes 786440 | tf_op jit(solution)/shard_map/ppermute | solution.py:407
  174.6 8.8 %collective-permute-start.12 = (bf16[128,1024]{1,0:T(8,128)(2,1)S(1)}, bf16[128,1024]{1,0:T(8,128)(2,1)S(1)}, u32[]{:S(2)}, u32[]{:S(2)}) collective-permute-start(bf16[128,1024]{1,0:T(8,128)(2,1)S(1)} %get-tuple-element.26), channel_id=1, source_target_pairs={{0,3},{3,0},{1,2},{2,1},{4,7},{7,4},{5,6},{6,5},{8,11},{11,8},{9,1... | collective-permute-start | bytes 786440 | tf_op jit(solution)/shard_map/ppermute | solution.py:411
  182.1 1.3 copy-start.11
  183.4 0.7 copy-start.12
Sparse Core Ops, SparseCore 0:
  10.1 106.6 all-gather.1

commit v2 on v1

v2 whole, which is shorter than its diff:
```python
import jax
import jax.numpy as jnp
from jax import lax
from jax.experimental import pallas as pl
from jax.experimental.pallas import tpu as pltpu
from jax.sharding import Mesh
from jax.sharding import PartitionSpec as P

HEADS = 32
HEAD_DIM = 64
GROUPS = 4
STATE = 128
CONV = 4
FCONV = 3
BLOCK = 128
SP = ("sp_0", "sp_1", "sp_2")
SP_TP = ("sp_0", "sp_1", "sp_2", "tp")

EPSILON = 1e-05
ALPHA = 2.0**0.25
F32 = jnp.float32
BF16 = jnp.bfloat16
NEG = -1e30

ROWS = 512
CH = 512
NH = 8
QUARTER = 128
HALFCH = 256
D = 2048
HALF = 1024
FFL = 1408

VMEM = pl.BlockSpec(memory_space=pltpu.VMEM)
SMEM = pl.BlockSpec(memory_space=pltpu.SMEM)
ANY = pl.BlockSpec(memory_space=pl.ANY)
HIGHEST = lax.Precision.HIGHEST


def dot(a, b):
    return jnp.dot(a, b, preferred_element_type=F32)


def dot_nt(a, b, precision=None):
    return lax.dot_general(
        a, b, (((1,), (1,)), ((), ())), precision=precision, preferred_element_type=F32
    )


def silu(v):
    return v / (1.0 + jnp.exp(-v))


def lane_pairs(column_of, rows):
    low = lax.broadcasted_iota(jnp.int32, (rows, 128), 1) < HEAD_DIM
    slabs = []
    for q in range(NH // 2):
        first = jnp.broadcast_to(column_of[:, 2 * q : 2 * q + 1], (rows, 128))
        second = jnp.broadcast_to(column_of[:, 2 * q + 1 : 2 * q + 2], (rows, 128))
        slabs.append(jnp.where(low, first, second))
    return slabs


def eye(n):
    line = lax.broadcasted_iota(jnp.int32, (n, n), 0)
    lane = lax.broadcasted_iota(jnp.int32, (n, n), 1)
    return jnp.where(line == lane, 1.0, 0.0).astype(F32)


def columns(rows):
    return dot_nt(eye(BLOCK), rows, precision=HIGHEST)


def decays(delta_ref, extra_ref, offset_ref, speed_ref):
    small = eye(NH)
    offset = jnp.sum(small * offset_ref[...], axis=1, keepdims=True)
    speed = jnp.sum(small * speed_ref[...], axis=1, keepdims=True)
    step_in = delta_ref[...] + offset
    step = jnp.maximum(step_in, 0.0) + jnp.log1p(jnp.exp(-jnp.abs(step_in)))
    return step, extra_ref[...] - speed * step


def running_sum(fading):
    line = lax.broadcasted_iota(jnp.int32, (BLOCK, BLOCK), 0)
    lane = lax.broadcasted_iota(jnp.int32, (BLOCK, BLOCK), 1)
    upper = jnp.where(line <= lane, 1.0, 0.0).astype(F32)
    return jnp.dot(fading, upper, precision=HIGHEST, preferred_element_type=F32)


def conv_at(pad, taps, start):
    total = None
    for k in range(CONV):
        term = taps[k : k + 1, :].astype(F32) * pad[pl.ds(start + 8 - CONV + 1 + k, BLOCK), :]
        total = term if total is None else total + term
    return silu(total)


def rim_kernel(x_ref, b_ref, c_ref, out_ref):
    out_ref[:, 0:CH] = x_ref[...]
    out_ref[:, CH : CH + STATE] = b_ref[...]
    out_ref[:, CH + STATE : CH + 2 * STATE] = c_ref[...]


def run_rim(x, b, c):
    last = lambda width: pl.BlockSpec((8, width), lambda i: (ROWS // 8 - 1, 0))
    return pl.pallas_call(
        rim_kernel,
        grid=(1,),
        out_shape=jax.ShapeDtypeStruct((8, CH + 2 * STATE), BF16),
        in_specs=[last(CH), last(STATE), last(STATE)],
        out_specs=pl.BlockSpec((8, CH + 2 * STATE), lambda i: (0, 0)),
        name="rim",
    )(x, b, c)


def state_kernel(
    x_ref, b_ref, rim_ref, xt_ref, bt_ref, delta_ref, extra_ref, offset_ref, speed_ref,
    x_out, b_out, state_out, msg_ref,
    xpad, bpad,
):
    xpad[0:8, :] = rim_ref[:, 0:CH].astype(F32)
    bpad[0:8, :] = rim_ref[:, CH : CH + STATE].astype(F32)
    xpad[8 : 8 + ROWS, :] = x_ref[...].astype(F32)
    bpad[8 : 8 + ROWS, :] = b_ref[...].astype(F32)
    step, fading = decays(delta_ref, extra_ref, offset_ref, speed_ref)
    state = [jnp.zeros((STATE, 128), F32) for _ in range(NH // 2)]
    base = jnp.zeros((NH, 1), F32)
    for i in range(ROWS // BLOCK):
        start = i * BLOCK
        rows = pl.ds(start, BLOCK)
        here = slice(start, start + BLOCK)
        cum = running_sum(fading[:, here])
        last = cum[:, BLOCK - 1 : BLOCK]
        to_end = lane_pairs(columns(step[:, here] * jnp.exp(last - cum)), BLOCK)
        kept = lane_pairs(columns(jnp.broadcast_to(jnp.exp(last), (NH, BLOCK)))[0:1, :], 1)
        x_act = conv_at(xpad, xt_ref, start).astype(BF16)
        b_act = conv_at(bpad, bt_ref, start).astype(BF16)
        x_out[rows, :] = x_act
        b_out[rows, :] = b_act
        b_turned = b_act.astype(F32).T.astype(BF16)
        for q in range(NH // 2):
            cols = slice(q * 128, (q + 1) * 128)
            fresh = dot(b_turned, (x_act[:, cols].astype(F32) * to_end[q]).astype(BF16))
            state[q] = fresh if i == 0 else state[q] * kept[q] + fresh
            if i < ROWS // BLOCK - 1:
                state_out[i, :, cols] = state[q].astype(BF16)
        base = base + last
    totals = lane_pairs(columns(jnp.broadcast_to(base, (NH, BLOCK)))[0:1, :], 1)
    for q in range(NH // 2):
        block = slice(q * 16, (q + 1) * 16)
        msg_ref[block, 0:8, :] = state[q].reshape(16, 8, 128).astype(BF16)
        left = totals[q]
        parts = []
        for _ in range(3):
            part = left.astype(BF16)
            parts.append(part.astype(F32))
            left = left - part.astype(F32)
        line = lax.broadcasted_iota(jnp.int32, (8, 128), 0)
        packed = jnp.where(line == 0, parts[0], jnp.where(line == 1, parts[1], parts[2]))
        packed = jnp.where(line < 3, packed, 0.0).astype(BF16)
        msg_ref[block, 8:16, :] = jnp.broadcast_to(packed[None], (16, 8, 128))


def run_state(x, b, rim, xt, bt, delta, extra, offset, speed):
    return pl.pallas_call(
        state_kernel,
        out_shape=(
            jax.ShapeDtypeStruct((ROWS, CH), BF16),
            jax.ShapeDtypeStruct((ROWS, STATE), BF16),
            jax.ShapeDtypeStruct((ROWS // BLOCK - 1, STATE, CH), BF16),
            jax.ShapeDtypeStruct((64, 16, 128), BF16),
        ),
        in_specs=[VMEM] * 9,
        out_specs=(VMEM,) * 4,
        scratch_shapes=[
            pltpu.VMEM((ROWS + 8, CH), F32),
            pltpu.VMEM((ROWS + 8, STATE), F32),
        ],
        name="local_state",
    )(x, b, rim, xt, bt, delta, extra, offset, speed)


def local_kernel(
    x_ref, b_ref, state_ref, c_ref, rim_ref, ct_ref, delta_ref, extra_ref, offset_ref, speed_ref,
    bypass_ref,
    y_ref, cact_ref, grow_ref,
    cpad,
):
    cpad[0:8, :] = rim_ref[:, CH + STATE : CH + 2 * STATE].astype(F32)
    cpad[8 : 8 + ROWS, :] = c_ref[...].astype(F32)
    step, fading = decays(delta_ref, extra_ref, offset_ref, speed_ref)
    bypass = lane_pairs(bypass_ref[...], 1)
    row = lax.broadcasted_iota(jnp.int32, (BLOCK, BLOCK), 0)
    col = lax.broadcasted_iota(jnp.int32, (BLOCK, BLOCK), 1)
    causal = row >= col
    low = col < HEAD_DIM
    base = jnp.zeros((NH, 1), F32)
    for i in range(ROWS // BLOCK):
        start = i * BLOCK
        rows = pl.ds(start, BLOCK)
        here = slice(start, start + BLOCK)
        cum = running_sum(fading[:, here])
        turned = columns(jnp.concatenate([cum, jnp.exp(cum), jnp.exp(base + cum)], axis=0))
        grow_ref[rows, :] = turned[:, 2 * NH : 3 * NH]
        grown = lane_pairs(turned[:, NH : 2 * NH], BLOCK)
        c_act = conv_at(cpad, ct_ref, start).astype(BF16)
        cact_ref[rows, :] = c_act
        affinity = dot_nt(c_act, b_ref[rows, :])
        for q in range(NH // 2):
            cols = slice(q * 128, (q + 1) * 128)
            x_here = x_ref[rows, cols]
            within = []
            for h in (2 * q, 2 * q + 1):
                between = turned[:, h : h + 1] - cum[h : h + 1, :]
                lag = jnp.exp(jnp.where(causal, between, NEG)) * step[h : h + 1, here]
                within.append(dot((affinity * lag).astype(BF16), x_here))
            total = jnp.where(low, within[0], within[1]) + bypass[q] * x_here.astype(F32)
            if i > 0:
                total = total + dot(c_act, state_ref[i - 1, :, cols]) * grown[q]
            y_ref[rows, cols] = total
        base = base + cum[:, BLOCK - 1 : BLOCK]


def run_local(x, b, states, c, rim, ct, delta, extra, offset, speed, bypass):
    return pl.pallas_call(
        local_kernel,
        out_shape=(
            jax.ShapeDtypeStruct((ROWS, CH), F32),
            jax.ShapeDtypeStruct((ROWS, STATE), BF16),
            jax.ShapeDtypeStruct((ROWS, NH), F32),
        ),
        in_specs=[VMEM] * 11,
        out_specs=(VMEM,) * 3,
        scratch_shapes=[pltpu.VMEM((ROWS + 8, STATE), F32)],
        name="local_mixer",
    )(x, b, states, c, rim, ct, delta, extra, offset, speed, bypass)


def prefix_kernel(in_ref, out_ref):
    entering = jnp.zeros((8, 128), F32)
    for j in range(64):
        out_ref[j] = entering.astype(BF16)
        piece = in_ref[j].astype(F32)
        total = piece[8:9, :] + piece[9:10, :] + piece[10:11, :]
        entering = entering * jnp.exp(total) + piece[0:8, :]


def run_prefix(received):
    return pl.pallas_call(
        prefix_kernel,
        out_shape=jax.ShapeDtypeStruct((64, 8, 128), BF16),
        in_specs=[VMEM],
        out_specs=VMEM,
        name="state_prefix",
    )(received)


def gate_kernel(y_ref, cact_ref, grow_ref, in_ref, valve_ref, scale_ref, out_l, out_r):
    for i in range(ROWS // BLOCK):
        rows = pl.ds(i * BLOCK, BLOCK)
        grown = lane_pairs(grow_ref[rows, :], BLOCK)
        c_act = cact_ref[rows, :]
        gated = []
        square = jnp.zeros((BLOCK, 1), F32)
        for q in range(NH // 2):
            cols = slice(q * 128, (q + 1) * 128)
            entering = in_ref[q * 16 : (q + 1) * 16].astype(F32).reshape(STATE, 128).astype(BF16)
            y = y_ref[rows, cols] + dot(c_act, entering) * grown[q]
            y = y * silu(valve_ref[rows, cols].astype(F32))
            gated.append(y)
            square = square + jnp.sum(y * y, axis=-1, keepdims=True)
        factor = lax.rsqrt(square * (1.0 / CH) + EPSILON)
        for q in range(NH // 2):
            cols = slice(q * 128, (q + 1) * 128)
            half = (out_l, out_r)[q // 2]
            half[rows, (q % 2) * 128 : (q % 2 + 1) * 128] = (
                gated[q] * factor * scale_ref[0:1, cols]
            ).astype(BF16)


def run_gate(y, cact, grow, entering, valve, scale):
    return pl.pallas_call(
        gate_kernel,
        out_shape=(jax.ShapeDtypeStruct((ROWS, HALFCH), BF16),) * 2,
        in_specs=[VMEM] * 6,
        out_specs=(VMEM,) * 2,
        name="gate_norm",
    )(y, cact, grow, entering, valve, scale)


RIM = 16
CHUNK = 512


def project_kernel(
    place_ref, scale_ref, own_w, near_w, far_w, across_w, near_x, far_x, across_x,
    own_l, own_r, near_l, near_r, far_l, far_r, across_l, across_r,
    own_res, near_res, far_res, across_res,
    out_ref, tail_ref,
    weight, acts, res, total, w_sems, a_sems, r_sems,
):
    core = place_ref[4]
    mine = pl.ds(pl.multiple_of(core * HALF, HALF), HALF)
    other = pl.ds(pl.multiple_of((1 - core) * HALF, HALF), HALF)
    started = []

    def start(source, target, sem):
        copy = pltpu.make_async_copy(source, target, sem)
        copy.start()
        return copy

    act_copies = []
    lefts = (own_l, near_l, far_l, across_l)
    rights = (own_r, near_r, far_r, across_r)
    for k in range(4):
        at = k * CH
        act_copies.append(start(lefts[k], acts.at[:, at : at + HALFCH], a_sems.at[2 * k]))
        act_copies.append(
            start(rights[k], acts.at[:, at + HALFCH : at + CH], a_sems.at[2 * k + 1])
        )
    for n in range(D // CHUNK):
        cols = slice(n * CHUNK, (n + 1) * CHUNK)
        started.append(start(own_w.at[:, cols], weight.at[0:CH, cols], w_sems.at[n]))
    for k, (first, second) in enumerate(((near_w, near_x), (far_w, far_x), (across_w, across_x))):
        block = slice((k + 1) * CH, (k + 2) * CH)
        started.append(start(first, weight.at[block, mine], w_sems.at[4 + 2 * k]))
        started.append(start(second, weight.at[block, other], w_sems.at[5 + 2 * k]))
    res_copies = []
    for k, source in enumerate((own_res, near_res, far_res, across_res)):
        rows = pl.ds(pl.multiple_of(place_ref[k] * QUARTER, QUARTER), QUARTER)
        res_copies.append(start(source, res.at[rows, :], r_sems.at[k]))
    for copy in act_copies + started:
        copy.wait()
    for n in range(D // CHUNK):
        cols = slice(n * CHUNK, (n + 1) * CHUNK)
        total[:, cols] = dot(acts[...], weight[:, cols])
    for copy in res_copies:
        copy.wait()
    for i in range(ROWS // 64):
        rows = slice(i * 64, (i + 1) * 64)
        values = total[rows, :] + ALPHA * res[rows, :].astype(F32)
        centred = values - jnp.sum(values, axis=-1, keepdims=True) * (1.0 / D)
        spread = jnp.sum(centred * centred, axis=-1, keepdims=True) * (1.0 / D)
        normed = (centred * lax.rsqrt(spread + EPSILON) * scale_ref[...]).astype(BF16)
        out_ref[rows, :] = normed
        if i == ROWS // 64 - 1:
            tail_ref[...] = normed[64 - RIM :, :]


def run_project(place, scale, weights, acts, residuals):
    return pl.pallas_call(
        project_kernel,
        out_shape=(
            jax.ShapeDtypeStruct((ROWS, D), BF16),
            jax.ShapeDtypeStruct((RIM, D), BF16),
        ),
        in_specs=[SMEM, VMEM] + [ANY] * 19,
        out_specs=(VMEM, VMEM),
        scratch_shapes=[
            pltpu.VMEM((D, D), BF16),
            pltpu.VMEM((ROWS, D), BF16),
            pltpu.VMEM((ROWS, D), BF16),
            pltpu.VMEM((ROWS, D), F32),
            pltpu.SemaphoreType.DMA((10,)),
            pltpu.SemaphoreType.DMA((8,)),
            pltpu.SemaphoreType.DMA((4,)),
        ],
        compiler_params=pltpu.CompilerParams(vmem_limit_bytes=48 * 1024 * 1024),
        name="project_norm",
    )(place, scale, *weights, *acts, *residuals)


TILES = FFL // 128
NARROW = 512


def down_copies(w_ref, down, sems):
    return [
        pltpu.make_async_copy(
            w_ref.at[n * NARROW : (n + 1) * NARROW, 2 * FFL : 3 * FFL],
            down.at[n * NARROW : (n + 1) * NARROW, :],
            sems.at[n],
        )
        for n in range(D // NARROW)
    ]


def two_quarters(hid, place_ref, half):
    def rows_of(k):
        return hid[pl.ds(pl.multiple_of(place_ref[half, k] * QUARTER, QUARTER), QUARTER), :]

    return jnp.concatenate([rows_of(0), rows_of(1)], axis=0)


def widen_kernel(
    sent_ref, gate_t, up_t, normed, rim, w_ref,
    hid_out, send_l, send_r,
    rows, wide, down, hid, gate_pad, up_pad, row_sems, wide_sems, down_sems, out_sem,
):
    row_copies = [
        pltpu.make_async_copy(rim, rows.at[0:RIM, :], row_sems.at[0]),
        pltpu.make_async_copy(normed, rows.at[RIM : RIM + ROWS, :], row_sems.at[1]),
    ]

    def wide_copies(j):
        at = j * 128
        if not isinstance(j, int):
            at = pl.multiple_of(at, 128)
        return (
            pltpu.make_async_copy(
                w_ref.at[:, pl.ds(at, 128)], wide.at[j, :, 0:128], wide_sems.at[j, 0]
            ),
            pltpu.make_async_copy(
                w_ref.at[:, pl.ds(FFL + at, 128)], wide.at[j, :, 128:256], wide_sems.at[j, 1]
            ),
        )

    downs = down_copies(w_ref, down, down_sems)
    for copy in row_copies:
        copy.start()
    for j in range(TILES):
        for copy in wide_copies(j):
            copy.start()
    for copy in downs:
        copy.start()
    for copy in row_copies:
        copy.wait()

    def conv(pad, taps, at):
        total = None
        for k in range(FCONV):
            tap = taps[k : k + 1, pl.ds(at, 128)].astype(F32)
            term = tap * pad[pl.ds(RIM - FCONV + 1 + k, ROWS), :]
            total = term if total is None else total + term
        return total

    def tile(j, carry):
        for copy in wide_copies(j):
            copy.wait()
        at = pl.multiple_of(j * 128, 128)
        both = dot(rows[...], wide[j]).astype(BF16).astype(F32)
        gate_pad[...] = both[:, 0:128]
        up_pad[...] = both[:, 128:256]
        hid[:, pl.ds(at, 128)] = (
            silu(conv(gate_pad, gate_t, at)) * conv(up_pad, up_t, at)
        ).astype(BF16)
        return carry

    lax.fori_loop(0, TILES, tile, 0)
    stored = pltpu.make_async_copy(hid, hid_out, out_sem)
    stored.start()
    for copy in downs:
        copy.wait()
    send_l[...] = dot_nt(two_quarters(hid, sent_ref, 0), down[0:HALF, :]).astype(BF16)
    send_r[...] = dot_nt(two_quarters(hid, sent_ref, 1), down[HALF:D, :]).astype(BF16)
    stored.wait()


def run_widen(sent, normed, rim, weights, gate_t, up_t):
    return pl.pallas_call(
        widen_kernel,
        out_shape=(
            jax.ShapeDtypeStruct((ROWS, FFL), BF16),
            jax.ShapeDtypeStruct((2 * QUARTER, HALF), BF16),
            jax.ShapeDtypeStruct((2 * QUARTER, HALF), BF16),
        ),
        in_specs=[SMEM, VMEM, VMEM, ANY, ANY, ANY],
        out_specs=(ANY, VMEM, VMEM),
        scratch_shapes=[
            pltpu.VMEM((ROWS + RIM, D), BF16),
            pltpu.VMEM((TILES, D, 256), BF16),
            pltpu.VMEM((D, FFL), BF16),
            pltpu.VMEM((ROWS, FFL), BF16),
            pltpu.VMEM((ROWS + RIM, 128), F32),
            pltpu.VMEM((ROWS + RIM, 128), F32),
            pltpu.SemaphoreType.DMA((2,)),
            pltpu.SemaphoreType.DMA((TILES, 2)),
            pltpu.SemaphoreType.DMA((D // NARROW,)),
            pltpu.SemaphoreType.DMA,
        ],
        compiler_params=pltpu.CompilerParams(vmem_limit_bytes=48 * 1024 * 1024),
        name="widen",
    )(sent, gate_t, up_t, normed, rim, weights)


def held_kernel(
    held_ref, hid_ref, w_ref, own_l, pass_l, own_r, pass_r, hid, down, hid_sem, down_sems
):
    copies = [pltpu.make_async_copy(hid_ref, hid, hid_sem)] + down_copies(w_ref, down, down_sems)
    for copy in copies:
        copy.start()
    for copy in copies:
        copy.wait()
    left = dot_nt(two_quarters(hid, held_ref, 0), down[0:HALF, :])
    own_l[...] = left[0:QUARTER, :]
    pass_l[...] = left[QUARTER:, :]
    right = dot_nt(two_quarters(hid, held_ref, 1), down[HALF:D, :])
    own_r[...] = right[0:QUARTER, :]
    pass_r[...] = right[QUARTER:, :]


def run_held(held, hidden, weights):
    return pl.pallas_call(
        held_kernel,
        out_shape=(jax.ShapeDtypeStruct((QUARTER, HALF), F32),) * 4,
        in_specs=[SMEM, ANY, ANY],
        out_specs=(VMEM,) * 4,
        scratch_shapes=[
            pltpu.VMEM((ROWS, FFL), BF16),
            pltpu.VMEM((D, FFL), BF16),
            pltpu.SemaphoreType.DMA,
            pltpu.SemaphoreType.DMA((D // NARROW,)),
        ],
        name="shrink_held",
    )(held, hidden, weights)


def add_kernel(pass_l, pass_r, once_l, once_r, out_l, out_r):
    out_l[...] = (pass_l[...] + once_l[...].astype(F32)).astype(BF16)
    out_r[...] = (pass_r[...] + once_r[...].astype(F32)).astype(BF16)


def run_add(passes, onces):
    step = QUARTER // 2
    block = pl.BlockSpec((step, HALF), lambda i: (i, 0))
    lower = pl.BlockSpec((step, HALF), lambda i: (i + 2, 0))
    return pl.pallas_call(
        add_kernel,
        grid=(2,),
        out_shape=(jax.ShapeDtypeStruct((QUARTER, HALF), BF16),) * 2,
        in_specs=[block, block, lower, lower],
        out_specs=(block, block),
        name="round_sum",
    )(*passes, *onces)


def last_norm_kernel(
    place_ref, own_l, own_r, once_l, once_r, twice_l, twice_r, res_ref, scale_ref, out_ref
):
    left = own_l[...] + once_l[...].astype(F32) + twice_l[...].astype(F32)
    right = own_r[...] + once_r[...].astype(F32) + twice_r[...].astype(F32)
    left = left + ALPHA * res_ref[:, 0:HALF].astype(F32)
    right = right + ALPHA * res_ref[:, HALF:D].astype(F32)
    mean = (jnp.sum(left, axis=-1, keepdims=True) + jnp.sum(right, axis=-1, keepdims=True)) * (
        1.0 / D
    )
    left = left - mean
    right = right - mean
    spread = (
        jnp.sum(left * left, axis=-1, keepdims=True)
        + jnp.sum(right * right, axis=-1, keepdims=True)
    ) * (1.0 / D)
    factor = lax.rsqrt(spread + EPSILON)
    out_ref[:, 0:HALF] = (left * factor * scale_ref[0:1, 0:HALF]).astype(BF16)
    out_ref[:, HALF:D] = (right * factor * scale_ref[0:1, HALF:D]).astype(BF16)


def run_last_norm(place, owns, onces, twices, normed, scale):
    step = QUARTER // 2
    block = pl.BlockSpec((step, HALF), lambda i, p: (i, 0))
    return pl.pallas_call(
        last_norm_kernel,
        grid_spec=pltpu.PrefetchScalarGridSpec(
            num_scalar_prefetch=1,
            grid=(2,),
            in_specs=[block] * 6
            + [
                pl.BlockSpec((step, D), lambda i, p: (2 * p[0] + i, 0)),
                pl.BlockSpec((1, D), lambda i, p: (0, 0)),
            ],
            out_specs=pl.BlockSpec((step, D), lambda i, p: (i, 0)),
        ),
        out_shape=jax.ShapeDtypeStruct((QUARTER, D), BF16),
        name="last_norm",
    )(place, *owns, *onces, *twices, normed, scale)


NEAR = [(0, 1), (1, 0), (2, 3), (3, 2)]
FAR = [(0, 3), (3, 0), (1, 2), (2, 1)]
ACROSS = [(0, 2), (2, 0), (1, 3), (3, 1)]


def with_near(part):
    return lax.ppermute(part, "tp", NEAR)


def with_far(part):
    return lax.ppermute(part, "tp", FAR)


def with_across(part):
    return lax.ppermute(part, "tp", ACROSS)


def with_core(part):
    return lax.ppermute(part, "sp_2", [(0, 1), (1, 0)])


def next_positions(shard):
    count = lax.axis_size(SP)
    return lax.ppermute(shard, SP, [(i, i + 1) for i in range(count - 1)])


def shards(
    incoming_residual_stream,
    result_valve,
    channel_feed_matrix,
    memory_feed_matrix,
    memory_query_matrix,
    unsoftened_deltas,
    delta_offset,
    channel_fading_speed,
    extra_log_fading,
    bypass_factor,
    channel_feed_kernel,
    memory_feed_kernel,
    memory_query_kernel,
    cluster_scaling_vector,
    mixer_result_matrix,
    initial_scaling_vector,
    valve_matrix,
    widen_matrix,
    shrink_matrix,
    valve_filter_kernel,
    widen_filter_kernel,
    latter_scaling_vector,
):
    own = lax.axis_index("tp").astype(jnp.int32)
    core = lax.axis_index("sp_2").astype(jnp.int32)
    near = own ^ 1
    far = 3 - own
    across = own ^ 2
    place = jnp.stack([own, near, far, across, core])
    sent = jnp.stack([jnp.stack([near, across]), jnp.stack([far, across])])
    held = jnp.stack([jnp.stack([own, far]), jnp.stack([own, near])])

    weights = lax.all_gather(
        jnp.concatenate([valve_matrix, widen_matrix, shrink_matrix.T], axis=1), SP, tiled=True
    )

    rim = next_positions(run_rim(channel_feed_matrix, memory_feed_matrix, memory_query_matrix))
    drives = (
        unsoftened_deltas.T,
        extra_log_fading.T,
        delta_offset.reshape(1, NH),
        channel_fading_speed.reshape(1, NH),
    )
    x_act, b_act, states, message = run_state(
        channel_feed_matrix,
        memory_feed_matrix,
        rim,
        channel_feed_kernel,
        memory_feed_kernel,
        *drives,
    )
    received = lax.all_to_all(message, SP, 0, 0, tiled=True)

    w_half = lax.dynamic_slice(mixer_result_matrix, (0, core * HALF), (CH, HALF))
    w_mine = (with_near(w_half), with_far(w_half), with_across(w_half))
    w_other = tuple(with_core(part) for part in w_mine)
    residuals = (
        incoming_residual_stream,
        with_near(incoming_residual_stream),
        with_far(incoming_residual_stream),
        with_across(incoming_residual_stream),
    )

    y_local, c_act, grow = run_local(
        x_act,
        b_act,
        states,
        memory_query_matrix,
        rim,
        memory_query_kernel,
        *drives,
        bypass_factor.reshape(1, NH),
    )
    entering = lax.all_to_all(run_prefix(received), SP, 0, 0, tiled=True)
    y_l, y_r = run_gate(
        y_local, c_act, grow, entering, result_valve, cluster_scaling_vector.reshape(1, CH)
    )
    far_l = with_far(y_l)
    near_r = with_near(y_r)
    near_l = with_near(y_l)
    far_r = with_far(y_r)
    across_l = with_near(far_l)
    across_r = with_far(near_r)
    normed, tail = run_project(
        place,
        initial_scaling_vector.reshape(1, D),
        (mixer_result_matrix, *w_mine, *w_other),
        (y_l, y_r, near_l, near_r, far_l, far_r, across_l, across_r),
        residuals,
    )
    hidden, send_l, send_r = run_widen(
        sent, normed, next_positions(tail), weights, valve_filter_kernel, widen_filter_kernel
    )
    onces = (with_near(send_l), with_far(send_r))
    own_l, pass_l, own_r, pass_r = run_held(held, hidden, weights)
    on_l, on_r = run_add((pass_l, pass_r), onces)
    twices = (with_far(on_l), with_near(on_r))
    return run_last_norm(
        place, (own_l, own_r), onces, twices, normed, latter_scaling_vector.reshape(1, D)
    )


def solution(mesh):
    split = Mesh(mesh.devices.reshape(8, 4, 2, mesh.shape["tp"]), ("sp_0", "sp_1", "sp_2", "tp"))
    in_specs = (
        P(SP_TP, None),
        P(SP, "tp"),
        P(SP, "tp"),
        P(SP, "tp"),
        P(SP, "tp"),
        P(SP, "tp"),
        P("tp"),
        P("tp"),
        P(SP, "tp"),
        P("tp"),
        P(None, "tp"),
        P(None, "tp"),
        P(None, "tp"),
        P("tp"),
        P("tp", None),
        P(),
        P(SP, "tp"),
        P(SP, "tp"),
        P("tp", SP),
        P(None, "tp"),
        P(None, "tp"),
        P(),
    )
    out_specs = P(SP_TP, None)
    return jax.shard_map(
        shards, mesh=split, in_specs=in_specs, out_specs=out_specs, check_vma=False
    )
```

time: 195 us -> 208 us (1.067)
  starting transfers between devices: 23.6 us -> 53.3 us
  blocking collectives: 26.6 us -> 0 us
  other arithmetic: 13 us -> 2.52 us
  Pallas kernels: 46.7 us -> 55.8 us
  waiting for transfers between devices: 59.3 us -> 68.3 us
  local copies, waits for them, and re-layouts: 11.2 us -> 13.9 us
    all_to_all x1 -> x0, blocking collectives: 26.6 us -> none  [shards(): received = lax.all_to_all(message, SP, 0, 0, tiled=True)]
    all_to_all x0 -> x1, starting transfers between devices: none -> 13.5 us  [shards(): received = lax.all_to_all(message, SP, 0, 0, tiled=True)]
    pallas_call x6 -> x8, Pallas kernels: 38.8 us -> 48.2 us  [the longest x1 13.9 us: run_widen(): pl.pallas_call(widen_kernel, out_shape=(jax.ShapeDtypeStruct((ROWS, FFL),...]
    ppermute x0 -> x5, starting transfers between devices: none -> 6.99 us  [the longest x2 4.78 us: with_across(): return lax.ppermute(part, 'tp', ACROSS)]
    all_to_all x1, starting transfers between devices: 5.19 us -> 11.6 us  [shards(): entering = lax.all_to_all(run_prefix(received), SP, 0, 0, tiled=True)]
    ppermute x6 -> x7, waiting for transfers between devices: 26.2 us -> 32.3 us  [with_near(): return lax.ppermute(part, 'tp', NEAR)]
    ppermute x6 -> x7, waiting for transfers between devices: 21.8 us -> 27.4 us  [with_far(): return lax.ppermute(part, 'tp', FAR)]
    unnamed x34 -> x40, local copies, waits for them, and re-layouts: 6.39 us -> 11.5 us
  transfers between devices with their start and end apart: 16 -> 24, of which waited for: 11 -> 11; matrix products, arithmetic and copies ran while one was open for 8% -> 1% of each run, Pallas kernels for 12% -> 18%
where the time goes in v2:
time: 208 us; the launch traced here: 207 us
  waiting for transfers between devices  68.3 us (33%)
  Pallas kernels  55.8 us (27%)
  starting transfers between devices  53.3 us (26%)
  local copies, waits for them, and re-layouts  13.9 us (7%)
  between operations  13.6 us (7%)
  other arithmetic  2.52 us (1%)
    ppermute x7, waiting for transfers between devices, with_near(): return lax.ppermute(part, 'tp', NEAR)  32.3 us
    ppermute x7, waiting for transfers between devices, with_far(): return lax.ppermute(part, 'tp', FAR)  27.4 us
    pallas_call x1, Pallas kernels, run_widen(): pl.pallas_call(widen_kernel, out_shape=(jax.ShapeDtypeStruct((ROWS, FFL),...  13.9 us
    all_to_all x1, starting transfers between devices, shards(): received = lax.all_to_all(message, SP, 0, 0, tiled=True)  13.5 us
    all_to_all x1, starting transfers between devices, shards(): entering = lax.all_to_all(run_prefix(received), SP, 0, 0, tiled=True)  11.6 us
    pallas_call x1, Pallas kernels, run_project(): pl.pallas_call(project_kernel, out_shape=(jax.ShapeDtypeStruct((ROWS, D),...  11.6 us
    unnamed x40, local copies, waits for them, and re-layouts  11.5 us
    ppermute x2, starting transfers between devices, next_positions(): return lax.ppermute(shard, SP, [(i, i + 1) for i in range(count - 1)])  10.2 us
  transfers between devices with their start and end apart: 24, of which 11 were waited for; matrix products, arithmetic and copies ran while one was open for 1% of the time, Pallas kernels for 18%

profile of v2, /device:TPU:1, one launch (start us, length us, event | category | flops | bytes accessed | tf_op | source)
XLA Modules:
  0.0 207.4 jit_solution(1681009500962746673)
XLA Ops:
  6.5 1.8 pad_maximum_fusion
  8.3 0.0 all-gather.2.cloned.1.call-update
  8.3 2.3 %constant_dynamic-slice_fusion = bf16[512,1024]{1,0:T(8,128)(2,1)} fusion(bf16[512,2048]{1,0:T(8,128)(2,1)} %own_w.1, s32[]{:T(128)S(6)} %select_n.3), kind=kLoop, calls=%fused_computation.7 | loop fusion | bytes 2097156 | tf_op jit(solution)/shard_map/dynamic_slice | solution.py:658
  10.6 2.1 %collective-permute-start = (bf16[512,1024]{1,0:T(8,128)(2,1)}, bf16[512,1024]{1,0:T(8,128)(2,1)S(1)}, u32[]{:S(2)}, u32[]{:S(2)}) collective-permute-start(bf16[512,1024]{1,0:T(8,128)(2,1)} %constant_dynamic-slice_fusion), channel_id=1, source_target_pairs={{0,1},{1,0},{2,3},{3,2},{4,5},{5,4},{6,7},{7,6},{8,9},{9,8},{10,11... | collective-permute-start | bytes 3145736 | tf_op jit(solution)/shard_map/ppermute | solution.py:584
  12.7 1.9 collective-permute-start.1
  14.6 0.7 collective-permute-start.2
  15.4 0.6 collective-permute-start.13
  16.0 1.3 rim.1
  17.3 4.8 %collective-permute-start.6 = (bf16[8,768]{1,0:T(8,128)(2,1)}, bf16[8,768]{1,0:T(8,128)(2,1)S(1)}, u32[]{:S(2)}, u32[]{:S(2)}) collective-permute-start(bf16[8,768]{1,0:T(8,128)(2,1)} %rim.1), channel_id=1, source_target_pairs={{0,4},{4,8},{8,12},{12,16},{16,20},{20,24},{24,28},{28,32},{32,36}... | collective-permute-start | bytes 36872 | tf_op jit(solution)/shard_map/ppermute | solution.py:601
  22.1 1.0 collective-permute-done.6.rim_ref
  23.1 0.6 copy-done.19
  23.7 5.7 %local_state.1 = (bf16[512,512]{1,0:T(8,128)(2,1)}, bf16[512,128]{1,0:T(8,128)(2,1)}, bf16[3,128,512]{2,1,0:T(8,128)(2,1)}, bf16[64,16,128]{2,1,0:T(8,128)(2,1)}) custom-call(bf16[512,512]{1,0:T(8,128)(2,1)} %x_ref.3, bf16[512,128]{1,0:T(8,128)(2,1)} %b_ref.3, bf16[8,768]{1,0:T(8,128)(2,1)} %copy-done.19, bf16[4,512]{1,0:T(4,128)(2,1)} %xt_ref.1, ...), custom_call_target="tpu_custom_call" | custom-call | tf_op jit(solution)/shard_map/local_state/pallas_call | solution.py:165
  29.4 13.5 %all-to-all-start = ((bf16[64,16,128]{2,1,0:T(8,128)(2,1)}), bf16[64,16,128]{2,1,0:T(8,128)(2,1)S(1)}, u32[]{:S(2)}, u32[]{:S(2)}) async-start(bf16[64,16,128]{2,1,0:T(8,128)(2,1)} %get-tuple-element.31), calls=%async_computation | async-start | bytes 524288 | tf_op jit(solution)/shard_map/all_to_all | solution.py:656
  43.0 0.0 copy-start.11
  43.0 2.0 collective-permute-start.14
  45.0 23.4 %collective-permute-done.13.near_res = bf16[128,2048]{1,0:T(8,128)(2,1)S(1)} collective-permute-done((bf16[128,2048]{1,0:T(8,128)(2,1)S(1)}, bf16[128,2048]{1,0:T(8,128)(2,1)S(1)}, u32[]{:S(2)}, u32[]{:S(2)}) %collective-permute-start.13) | collective-permute-done | bytes 524320 | tf_op jit(solution)/shard_map/ppermute | solution.py:584
  68.4 4.1 %collective-permute-start.15 = (bf16[128,2048]{1,0:T(8,128)(2,1)S(1)}, bf16[128,2048]{1,0:T(8,128)(2,1)S(1)}, u32[]{:S(2)}, u32[]{:S(2)}) collective-permute-start(bf16[128,2048]{1,0:T(8,128)(2,1)S(1)} %copy-done.2), channel_id=1, source_target_pairs={{0,2},{2,0},{1,3},{3,1},{4,6},{6,4},{5,7},{7,5},{8,10},{10,8},{9,1... | collective-permute-start | bytes 1572872 | tf_op jit(solution)/shard_map/ppermute | solution.py:592
  72.5 0.0 collective-permute-done.near_w
  72.5 1.7 collective-permute-start.3
  74.2 0.1 collective-permute-start.4
  74.3 0.4 collective-permute-start.5
  74.7 0.7 copy-done.15
  75.4 1.8 state_prefix.1
  77.2 11.6 %all-to-all-start.1 = ((bf16[64,8,128]{2,1,0:T(8,128)(2,1)}), bf16[64,8,128]{2,1,0:T(8,128)(2,1)S(1)}, u32[]{:S(2)}, u32[]{:S(2)}) async-start(bf16[64,8,128]{2,1,0:T(8,128)(2,1)} %state_prefix.1), calls=%async_computation.1 | async-start | bytes 262144 | tf_op jit(solution)/shard_map/all_to_all | solution.py:678
  88.8 5.9 %local_mixer.1 = (f32[512,512]{1,0:T(8,128)}, bf16[512,128]{1,0:T(8,128)(2,1)}, f32[512,8]{1,0:T(8,128)}) custom-call(bf16[512,512]{1,0:T(8,128)(2,1)} %get-tuple-element.25.x_ref, bf16[512,128]{1,0:T(8,128)(2,1)} %get-tuple-element.26.b_ref, bf16[3,128,512]{2,1,0:T(8,128)(2,1)} %get-tuple-element.27.state_ref, bf16[512,128]{1,0:T(8,128)(2,1)} %c_ref.3, ...), custom_call_target="tpu_custom_call" | custom-call | tf_op jit(solution)/shard_map/local_mixer/pallas_call | solution.py:225
  94.7 6.5 %all-to-all-done.1.in_ref = bf16[64,8,128]{2,1,0:T(8,128)(2,1)S(1)} async-done(((bf16[64,8,128]{2,1,0:T(8,128)(2,1)}), bf16[64,8,128]{2,1,0:T(8,128)(2,1)S(1)}, u32[]{:S(2)}, u32[]{:S(2)}) %all-to-all-start.1) | async-done | bytes 131104 | tf_op jit(solution)/shard_map/all_to_all | solution.py:678
  101.1 0.6 copy-done.16
  101.8 3.5 %gate_norm.1 = (bf16[512,256]{1,0:T(8,128)(2,1)}, bf16[512,256]{1,0:T(8,128)(2,1)}) custom-call(f32[512,512]{1,0:T(8,128)} %get-tuple-element.28.y_ref, bf16[512,128]{1,0:T(8,128)(2,1)} %get-tuple-element.29.cact_ref, f32[512,8]{1,0:T(8,128)} %get-tuple-element.30.grow_ref, bf16[64,8,128]{2,1,0:T(8,128)(2,1)} %copy-done.16, bf16[512,512]{1,0:T(8,128)(2,1)} %valve_ref.1, ...), custom_call_target="tpu_custom_call" | custom-call | tf_op jit(solution)/shard_map/gate_norm/pallas_call | solution.py:282
  105.3 0.8 collective-permute-start.9
  106.1 8.1 %collective-permute-done.9.far_l = bf16[512,256]{1,0:T(8,128)(2,1)S(1)} collective-permute-done((bf16[512,256]{1,0:T(8,128)(2,1)}, bf16[512,256]{1,0:T(8,128)(2,1)S(1)}, u32[]{:S(2)}, u32[]{:S(2)}) %collective-permute-start.9) | collective-permute-done | bytes 262176 | tf_op jit(solution)/shard_map/ppermute | solution.py:588
  114.2 0.8 collective-permute-start.10
  115.0 7.2 %collective-permute-done.10.far_r = bf16[512,256]{1,0:T(8,128)(2,1)S(1)} collective-permute-done((bf16[512,256]{1,0:T(8,128)(2,1)}, bf16[512,256]{1,0:T(8,128)(2,1)S(1)}, u32[]{:S(2)}, u32[]{:S(2)}) %collective-permute-start.10) | collective-permute-done | bytes 262176 | tf_op jit(solution)/shard_map/ppermute | solution.py:588
  122.3 0.7 copy-done.5
  123.0 0.7 copy-done.7
  123.7 0.9 collective-permute-start.12
  124.6 0.1 stack.61.place_ref
  124.7 0.1 add_bitcast_fusion.2
  124.7 4.2 %collective-permute-done.11.across_l = bf16[512,256]{1,0:T(8,128)(2,1)} collective-permute-done((bf16[512,256]{1,0:T(8,128)(2,1)S(1)}, bf16[512,256]{1,0:T(8,128)(2,1)}, u32[]{:S(2)}, u32[]{:S(2)}) %collective-permute-start.11) | collective-permute-done | bytes 262176 | tf_op jit(solution)/shard_map/ppermute | solution.py:584
  128.9 2.1 %collective-permute-done.12.across_r = bf16[512,256]{1,0:T(8,128)(2,1)} collective-permute-done((bf16[512,256]{1,0:T(8,128)(2,1)}, bf16[512,256]{1,0:T(8,128)(2,1)}, u32[]{:S(2)}, u32[]{:S(2)}) %collective-permute-start.12) | collective-permute-done | bytes 262176 | tf_op jit(solution)/shard_map/ppermute | solution.py:588
  131.1 0.0 copy-start.3
  131.1 0.9 copy-done.3
  132.0 0.9 copy-done.4
  133.0 0.9 copy-done.6
  133.9 0.9 copy-done.8
  134.9 11.6 %project_norm.1 = (bf16[512,2048]{1,0:T(8,128)(2,1)}, bf16[16,2048]{1,0:T(8,128)(2,1)S(1)}) custom-call(s32[5]{0:T(128)S(1)} %stack.61.place_ref, f32[1,2048]{1,0:T(1,128)S(1)} %bitcast.22, bf16[512,2048]{1,0:T(8,128)(2,1)} %own_w.1, bf16[512,1024]{1,0:T(8,128)(2,1)S(1)} %collective-permute-done.near_w, bf16[512,1024]{1,0:T(8,128)(2,1)} %collective-permute-done.1.far_w, ...), custom_call_target="tpu_custom_call" | custom-call | tf_op jit(solution)/shard_map/project_norm/pallas_call | solution.py:351
  146.5 5.4 %collective-permute-start.16 = (bf16[16,2048]{1,0:T(8,128)(2,1)S(1)}, bf16[16,2048]{1,0:T(8,128)(2,1)S(1)}, u32[]{:S(2)}, u32[]{:S(2)}) collective-permute-start(bf16[16,2048]{1,0:T(8,128)(2,1)S(1)} %get-tuple-element.35), channel_id=1, source_target_pairs={{0,4},{4,8},{8,12},{12,16},{16,20},{20,24},{24,28},{28,32},{32,36}... | collective-permute-start | bytes 196616 | tf_op jit(solution)/shard_map/ppermute | solution.py:601
  151.9 1.1 collective-permute-done.16.rim
  153.0 1.6 copy-done
  154.6 13.9 %widen.1 = (bf16[512,1408]{1,0:T(8,128)(2,1)S(1)}, bf16[256,1024]{1,0:T(8,128)(2,1)S(1)}, bf16[256,1024]{1,0:T(8,128)(2,1)S(1)}) custom-call(s32[2,2]{1,0:T(2,128)S(1)} %pad_add_fusion.1.sent_ref, bf16[3,1408]{1,0:T(4,128)(2,1)S(1)} %copy-done.9, bf16[3,1408]{1,0:T(4,128)(2,1)S(1)} %copy-done.10, bf16[512,2048]{1,0:T(8,128)(2,1)S(1)} %copy-done, ...), custom_call_target="tpu_custom_call" | custom-call | tf_op jit(solution)/shard_map/widen/pallas_call | solution.py:460
  168.5 1.1 copy-done.1
  169.6 0.3 collective-permute-start.17
  169.8 0.7 collective-permute-start.18
  170.6 0.1 add_bitcast_fusion
  170.6 0.6 pad_add_fusion.held_ref
  171.2 6.6 %shrink_held.1 = (f32[128,1024]{1,0:T(8,128)}, f32[128,1024]{1,0:T(8,128)}, f32[128,1024]{1,0:T(8,128)}, f32[128,1024]{1,0:T(8,128)}) custom-call(s32[2,2]{1,0:T(2,128)} %pad_add_fusion.held_ref, bf16[512,1408]{1,0:T(8,128)(2,1)} %copy-done.1, bf16[2048,4224]{1,0:T(8,128)(2,1)} %all-gather.2.cloned.1.call-done.w_ref), custom_call_target="tpu_custom_call" | custom-call | tf_op jit(solution)/shard_map/shrink_held/pallas_call | solution.py:503
  177.8 4.7 %collective-permute-done.17.once_l = bf16[256,1024]{1,0:T(8,128)(2,1)S(1)} collective-permute-done((bf16[256,1024]{1,0:T(8,128)(2,1)S(1)}, bf16[256,1024]{1,0:T(8,128)(2,1)S(1)}, u32[]{:S(2)}, u32[]{:S(2)}) %collective-permute-start.17) | collective-permute-done | bytes 524320 | tf_op jit(solution)/shard_map/ppermute | solution.py:584
  182.6 1.5 collective-permute-done.18.once_r
  184.0 0.8 copy-done.14
  184.8 2.1 %round_sum.1 = (bf16[128,1024]{1,0:T(8,128)(2,1)}, bf16[128,1024]{1,0:T(8,128)(2,1)}) custom-call(f32[128,1024]{1,0:T(8,128)} %get-tuple-element.41.pass_l, f32[128,1024]{1,0:T(8,128)} %get-tuple-element.42.pass_r, bf16[256,1024]{1,0:T(8,128)(2,1)} %copy-done.13, bf16[256,1024]{1,0:T(8,128)(2,1)} %copy-done.14), custom_call_target="tpu_custom_call" | custom-call | tf_op jit(solution)/shard_map/round_sum/pallas_call | solution.py:527
  186.9 0.8 collective-permute-start.19
  187.7 8.4 %collective-permute-done.19.twice_l = bf16[128,1024]{1,0:T(8,128)(2,1)S(1)} collective-permute-done((bf16[128,1024]{1,0:T(8,128)(2,1)}, bf16[128,1024]{1,0:T(8,128)(2,1)S(1)}, u32[]{:S(2)}, u32[]{:S(2)}) %collective-permute-start.19) | collective-permute-done | bytes 262176 | tf_op jit(solution)/shard_map/ppermute | solution.py:588
  196.2 0.7 copy-done.17
  196.9 0.1 copy-done.18
  197.0 3.5 %last_norm.1 = bf16[128,2048]{1,0:T(8,128)(2,1)} custom-call(s32[5]{0:T(128)} %copy-done.12, f32[128,1024]{1,0:T(8,128)} %get-tuple-element.37.own_l, f32[128,1024]{1,0:T(8,128)} %get-tuple-element.38.own_r, bf16[256,1024]{1,0:T(8,128)(2,1)} %copy-done.13, bf16[256,1024]{1,0:T(8,128)(2,1)} %copy-done.14, bf16[128,1024]{1,0:T(8,128)(2,1)} %copy-done.17, ...), custom_call_target="tpu_custom_call" | custom-call | tf_op jit(solution)/shard_map/last_norm/pallas_call | solution.py:561
  (42 shorter events, 0.1 us)
Async XLA Ops:
  6.5 8.8 %copy-start.2 = (bf16[128,2048]{1,0:T(8,128)(2,1)S(1)}, bf16[128,2048]{1,0:T(8,128)(2,1)}, u32[]{:S(2)}) copy-start(bf16[128,2048]{1,0:T(8,128)(2,1)} %own_res.1) | copy-start | bytes 1572868
  6.5 146.5 %all-gather.2.cloned.1.call-start = ((), (), s32[]{:S(2)}) async-start(), calls=%async_computation.2 | async-start | bytes 17571840 | tf_op jit(solution)/shard_map/all_gather | solution.py:637
  10.6 61.8 %collective-permute-start = (bf16[512,1024]{1,0:T(8,128)(2,1)}, bf16[512,1024]{1,0:T(8,128)(2,1)S(1)}, u32[]{:S(2)}, u32[]{:S(2)}) collective-permute-start(bf16[512,1024]{1,0:T(8,128)(2,1)} %constant_dynamic-slice_fusion), channel_id=1, source_target_pairs={{0,1},{1,0},{2,3},{3,2},{4,5},{5,4},{6,7},{7,6},{8,9},{9,8},{10,11... | collective-permute-start | bytes 3145736 | tf_op jit(solution)/shard_map/ppermute | solution.py:584
  12.7 61.4 %collective-permute-start.1 = (bf16[512,1024]{1,0:T(8,128)(2,1)}, bf16[512,1024]{1,0:T(8,128)(2,1)}, u32[]{:S(2)}, u32[]{:S(2)}) collective-permute-start(bf16[512,1024]{1,0:T(8,128)(2,1)} %constant_dynamic-slice_fusion), channel_id=1, source_target_pairs={{0,3},{3,0},{1,2},{2,1},{4,7},{7,4},{5,6},{6,5},{8,11},{11,8},{9,1... | collective-permute-start | bytes 3145736 | tf_op jit(solution)/shard_map/ppermute | solution.py:588
  14.6 59.6 %collective-permute-start.2 = (bf16[512,1024]{1,0:T(8,128)(2,1)}, bf16[512,1024]{1,0:T(8,128)(2,1)}, u32[]{:S(2)}, u32[]{:S(2)}) collective-permute-start(bf16[512,1024]{1,0:T(8,128)(2,1)} %constant_dynamic-slice_fusion), channel_id=1, source_target_pairs={{0,2},{2,0},{1,3},{3,1},{4,6},{6,4},{5,7},{7,5},{8,10},{10,8},{9,1... | collective-permute-start | bytes 3145736 | tf_op jit(solution)/shard_map/ppermute | solution.py:592
  15.4 53.0 %collective-permute-start.13 = (bf16[128,2048]{1,0:T(8,128)(2,1)S(1)}, bf16[128,2048]{1,0:T(8,128)(2,1)S(1)}, u32[]{:S(2)}, u32[]{:S(2)}) collective-permute-start(bf16[128,2048]{1,0:T(8,128)(2,1)S(1)} %copy-done.2), channel_id=1, source_target_pairs={{0,1},{1,0},{2,3},{3,2},{4,5},{5,4},{6,7},{7,6},{8,9},{9,8},{10,11... | collective-permute-start | bytes 1572872 | tf_op jit(solution)/shard_map/ppermute | solution.py:584
  17.3 5.8 %collective-permute-start.6 = (bf16[8,768]{1,0:T(8,128)(2,1)}, bf16[8,768]{1,0:T(8,128)(2,1)S(1)}, u32[]{:S(2)}, u32[]{:S(2)}) collective-permute-start(bf16[8,768]{1,0:T(8,128)(2,1)} %rim.1), channel_id=1, source_target_pairs={{0,4},{4,8},{8,12},{12,16},{16,20},{20,24},{24,28},{28,32},{32,36}... | collective-permute-start | bytes 36872 | tf_op jit(solution)/shard_map/ppermute | solution.py:601
  23.1 0.6 copy-start.19
  29.4 45.3 %all-to-all-start = ((bf16[64,16,128]{2,1,0:T(8,128)(2,1)}), bf16[64,16,128]{2,1,0:T(8,128)(2,1)S(1)}, u32[]{:S(2)}, u32[]{:S(2)}) async-start(bf16[64,16,128]{2,1,0:T(8,128)(2,1)} %get-tuple-element.31), calls=%async_computation | async-start | bytes 524288 | tf_op jit(solution)/shard_map/all_to_all | solution.py:656
  43.0 88.1 %copy-start.11 = (f32[2048]{0:T(1024)S(1)}, f32[2048]{0:T(1024)}, u32[]{:S(2)}) copy-start(f32[2048]{0:T(1024)} %param.37) | copy-start | bytes 24580
  43.0 62.3 %collective-permute-start.14 = (bf16[128,2048]{1,0:T(8,128)(2,1)S(1)}, bf16[128,2048]{1,0:T(8,128)(2,1)S(1)}, u32[]{:S(2)}, u32[]{:S(2)}) collective-permute-start(bf16[128,2048]{1,0:T(8,128)(2,1)S(1)} %copy-done.2), channel_id=1, source_target_pairs={{0,3},{3,0},{1,2},{2,1},{4,7},{7,4},{5,6},{6,5},{8,11},{11,8},{9,1... | collective-permute-start | bytes 1572872 | tf_op jit(solution)/shard_map/ppermute | solution.py:588
  68.4 37.7 %collective-permute-start.15 = (bf16[128,2048]{1,0:T(8,128)(2,1)S(1)}, bf16[128,2048]{1,0:T(8,128)(2,1)S(1)}, u32[]{:S(2)}, u32[]{:S(2)}) collective-permute-start(bf16[128,2048]{1,0:T(8,128)(2,1)S(1)} %copy-done.2), channel_id=1, source_target_pairs={{0,2},{2,0},{1,3},{3,1},{4,6},{6,4},{5,7},{7,5},{8,10},{10,8},{9,1... | collective-permute-start | bytes 1572872 | tf_op jit(solution)/shard_map/ppermute | solution.py:592
  72.5 58.6 %collective-permute-start.3 = (bf16[512,1024]{1,0:T(8,128)(2,1)S(1)}, bf16[512,1024]{1,0:T(8,128)(2,1)}, u32[]{:S(2)}, u32[]{:S(2)}) collective-permute-start(bf16[512,1024]{1,0:T(8,128)(2,1)S(1)} %collective-permute-done.near_w), channel_id=1, source_target_pairs={{0,4},{4,0},{1,5},{5,1},{2,6},{6,2},{3,7},{7,3},{8,12},{12,8},{9,1... | collective-permute-start | bytes 3145736 | tf_op jit(solution)/shard_map/ppermute | solution.py:596
  74.2 56.9 %collective-permute-start.4 = (bf16[512,1024]{1,0:T(8,128)(2,1)}, bf16[512,1024]{1,0:T(8,128)(2,1)}, u32[]{:S(2)}, u32[]{:S(2)}) collective-permute-start(bf16[512,1024]{1,0:T(8,128)(2,1)} %collective-permute-done.1.far_w), channel_id=1, source_target_pairs={{0,4},{4,0},{1,5},{5,1},{2,6},{6,2},{3,7},{7,3},{8,12},{12,8},{9,1... | collective-permute-start | bytes 3145736 | tf_op jit(solution)/shard_map/ppermute | solution.py:596
  74.3 56.8 %collective-permute-start.5 = (bf16[512,1024]{1,0:T(8,128)(2,1)}, bf16[512,1024]{1,0:T(8,128)(2,1)}, u32[]{:S(2)}, u32[]{:S(2)}) collective-permute-start(bf16[512,1024]{1,0:T(8,128)(2,1)} %collective-permute-done.2.across_w), channel_id=1, source_target_pairs={{0,4},{4,0},{1,5},{5,1},{2,6},{6,2},{3,7},{7,3},{8,12},{12,8},{9,1... | collective-permute-start | bytes 3145736 | tf_op jit(solution)/shard_map/ppermute | solution.py:596
  74.7 0.7 copy-start.15
  77.2 23.9 %all-to-all-start.1 = ((bf16[64,8,128]{2,1,0:T(8,128)(2,1)}), bf16[64,8,128]{2,1,0:T(8,128)(2,1)S(1)}, u32[]{:S(2)}, u32[]{:S(2)}) async-start(bf16[64,8,128]{2,1,0:T(8,128)(2,1)} %state_prefix.1), calls=%async_computation.1 | async-start | bytes 262144 | tf_op jit(solution)/shard_map/all_to_all | solution.py:678
  101.1 0.7 copy-start.16
  105.3 8.9 %collective-permute-start.9 = (bf16[512,256]{1,0:T(8,128)(2,1)}, bf16[512,256]{1,0:T(8,128)(2,1)S(1)}, u32[]{:S(2)}, u32[]{:S(2)}) collective-permute-start(bf16[512,256]{1,0:T(8,128)(2,1)} %get-tuple-element.32.own_l), channel_id=1, source_target_pairs={{0,3},{3,0},{1,2},{2,1},{4,7},{7,4},{5,6},{6,5},{8,11},{11,8},{9,1... | collective-permute-start | bytes 786440 | tf_op jit(solution)/shard_map/ppermute | solution.py:588
  106.1 9.0 %collective-permute-start.8 = (bf16[512,256]{1,0:T(8,128)(2,1)}, bf16[512,256]{1,0:T(8,128)(2,1)}, u32[]{:S(2)}, u32[]{:S(2)}) collective-permute-start(bf16[512,256]{1,0:T(8,128)(2,1)} %get-tuple-element.33.own_r), channel_id=1, source_target_pairs={{0,1},{1,0},{2,3},{3,2},{4,5},{5,4},{6,7},{7,6},{8,9},{9,8},{10,11... | collective-permute-start | bytes 786440 | tf_op jit(solution)/shard_map/ppermute | solution.py:584
  114.2 8.1 %collective-permute-start.10 = (bf16[512,256]{1,0:T(8,128)(2,1)}, bf16[512,256]{1,0:T(8,128)(2,1)S(1)}, u32[]{:S(2)}, u32[]{:S(2)}) collective-permute-start(bf16[512,256]{1,0:T(8,128)(2,1)} %get-tuple-element.33.own_r), channel_id=1, source_target_pairs={{0,3},{3,0},{1,2},{2,1},{4,7},{7,4},{5,6},{6,5},{8,11},{11,8},{9,1... | collective-permute-start | bytes 786440 | tf_op jit(solution)/shard_map/ppermute | solution.py:588
  115.0 8.0 %collective-permute-start.7 = (bf16[512,256]{1,0:T(8,128)(2,1)}, bf16[512,256]{1,0:T(8,128)(2,1)S(1)}, u32[]{:S(2)}, u32[]{:S(2)}) collective-permute-start(bf16[512,256]{1,0:T(8,128)(2,1)} %get-tuple-element.32.own_l), channel_id=1, source_target_pairs={{0,1},{1,0},{2,3},{3,2},{4,5},{5,4},{6,7},{7,6},{8,9},{9,8},{10,11... | collective-permute-start | bytes 786440 | tf_op jit(solution)/shard_map/ppermute | solution.py:584
  122.3 0.7 copy-start.5
  123.0 5.9 %collective-permute-start.11 = (bf16[512,256]{1,0:T(8,128)(2,1)S(1)}, bf16[512,256]{1,0:T(8,128)(2,1)}, u32[]{:S(2)}, u32[]{:S(2)}) collective-permute-start(bf16[512,256]{1,0:T(8,128)(2,1)S(1)} %collective-permute-done.9.far_l), channel_id=1, source_target_pairs={{0,1},{1,0},{2,3},{3,2},{4,5},{5,4},{6,7},{7,6},{8,9},{9,8},{10,11... | collective-permute-start | bytes 786440 | tf_op jit(solution)/shard_map/ppermute | solution.py:584
  123.0 0.7 copy-start.7
  123.7 7.3 %collective-permute-start.12 = (bf16[512,256]{1,0:T(8,128)(2,1)}, bf16[512,256]{1,0:T(8,128)(2,1)}, u32[]{:S(2)}, u32[]{:S(2)}) collective-permute-start(bf16[512,256]{1,0:T(8,128)(2,1)} %collective-permute-done.8.near_r), channel_id=1, source_target_pairs={{0,3},{3,0},{1,2},{2,1},{4,7},{7,4},{5,6},{6,5},{8,11},{11,8},{9,1... | collective-permute-start | bytes 786440 | tf_op jit(solution)/shard_map/ppermute | solution.py:588
  124.7 21.8 %copy-start.12 = (s32[5]{0:T(128)}, s32[5]{0:T(128)S(1)}, u32[]{:S(2)}) copy-start(s32[5]{0:T(128)S(1)} %stack.61.place_ref) | copy-start | bytes 64
  131.1 1.0 copy-start.3
  132.0 0.9 copy-start.4
  133.0 0.9 copy-start.6
  133.9 0.9 copy-start.8
  134.9 18.1 %copy-start.9 = (bf16[3,1408]{1,0:T(4,128)(2,1)S(1)}, bf16[3,1408]{1,0:T(4,128)(2,1)}, u32[]{:S(2)}) copy-start(bf16[3,1408]{1,0:T(4,128)(2,1)} %gate_t.1) | copy-start | bytes 25348
  134.9 18.1 %copy-start.10 = (bf16[3,1408]{1,0:T(4,128)(2,1)S(1)}, bf16[3,1408]{1,0:T(4,128)(2,1)}, u32[]{:S(2)}) copy-start(bf16[3,1408]{1,0:T(4,128)(2,1)} %up_t.1) | copy-start | bytes 25348
  146.5 6.5 %collective-permute-start.16 = (bf16[16,2048]{1,0:T(8,128)(2,1)S(1)}, bf16[16,2048]{1,0:T(8,128)(2,1)S(1)}, u32[]{:S(2)}, u32[]{:S(2)}) collective-permute-start(bf16[16,2048]{1,0:T(8,128)(2,1)S(1)} %get-tuple-element.35), channel_id=1, source_target_pairs={{0,4},{4,8},{8,12},{12,16},{16,20},{20,24},{24,28},{28,32},{32,36}... | collective-permute-start | bytes 196616 | tf_op jit(solution)/shard_map/ppermute | solution.py:601
  153.0 1.6 copy-start
  168.5 1.1 copy-start.1
  169.6 13.0 %collective-permute-start.17 = (bf16[256,1024]{1,0:T(8,128)(2,1)S(1)}, bf16[256,1024]{1,0:T(8,128)(2,1)S(1)}, u32[]{:S(2)}, u32[]{:S(2)}) collective-permute-start(bf16[256,1024]{1,0:T(8,128)(2,1)S(1)} %get-tuple-element.39), channel_id=1, source_target_pairs={{0,1},{1,0},{2,3},{3,2},{4,5},{5,4},{6,7},{7,6},{8,9},{9,8},{10,11... | collective-permute-start | bytes 1572872 | tf_op jit(solution)/shard_map/ppermute | solution.py:584
  169.8 14.2 %collective-permute-start.18 = (bf16[256,1024]{1,0:T(8,128)(2,1)S(1)}, bf16[256,1024]{1,0:T(8,128)(2,1)S(1)}, u32[]{:S(2)}, u32[]{:S(2)}) collective-permute-start(bf16[256,1024]{1,0:T(8,128)(2,1)S(1)} %get-tuple-element.40), channel_id=1, source_target_pairs={{0,3},{3,0},{1,2},{2,1},{4,7},{7,4},{5,6},{6,5},{8,11},{11,8},{9,1... | collective-permute-start | bytes 1572872 | tf_op jit(solution)/shard_map/ppermute | solution.py:588
  182.6 1.5 copy-start.13
  184.0 0.8 copy-start.14
  186.9 9.3 %collective-permute-start.19 = (bf16[128,1024]{1,0:T(8,128)(2,1)}, bf16[128,1024]{1,0:T(8,128)(2,1)S(1)}, u32[]{:S(2)}, u32[]{:S(2)}) collective-permute-start(bf16[128,1024]{1,0:T(8,128)(2,1)} %get-tuple-element.43), channel_id=1, source_target_pairs={{0,3},{3,0},{1,2},{2,1},{4,7},{7,4},{5,6},{6,5},{8,11},{11,8},{9,1... | collective-permute-start | bytes 786440 | tf_op jit(solution)/shard_map/ppermute | solution.py:588
  187.7 8.4 %collective-permute-start.20 = (bf16[128,1024]{1,0:T(8,128)(2,1)}, bf16[128,1024]{1,0:T(8,128)(2,1)S(1)}, u32[]{:S(2)}, u32[]{:S(2)}) collective-permute-start(bf16[128,1024]{1,0:T(8,128)(2,1)} %get-tuple-element.44), channel_id=1, source_target_pairs={{0,1},{1,0},{2,3},{3,2},{4,5},{5,4},{6,7},{7,6},{8,9},{9,8},{10,11... | collective-permute-start | bytes 786440 | tf_op jit(solution)/shard_map/ppermute | solution.py:584
  196.2 0.7 copy-start.17
  196.2 0.8 copy-start.18
Sparse Core Ops, SparseCore 0:
  10.1 110.0 all-gather.1
